TPU v7x, 32 devices: a whole 2x2x4 slice. The times are simulated.
32 devices in a mesh: rep: 2 (over x), fs: 8 (over z, y), tp: 2 (over core).
Axes of the slice: x: 2, y: 2, z: 4, core: 2. Of those that a mesh axis runs over, the one named last changes fastest.
Arguments:
- stream: bfloat16 [8192, 2048], P(('rep', 'fs'), 'tp'), may hold values from -6 to 6
- recurrent_norm_gain: float32 [2048], replicated, may hold values from 0.1 to 1.9
- feedforward_norm_gain: float32 [2048], replicated, may hold values from 0.1 to 1.9
- recurrent_input_weight: bfloat16 [2048, 2048], P('fs', 'tp'), may hold values from -0.125 to 0.125
- output_gate_weight: bfloat16 [2048, 2048], P('fs', 'tp'), may hold values from -0.125 to 0.125
- causal_filter_weight: bfloat16 [4, 2048], P(None, 'tp'), may hold values from -3 to 3
- decay_gate_matrix: bfloat16 [32, 64, 64], P('tp'), may hold values from -0.75 to 0.75
- input_gate_matrix: bfloat16 [32, 64, 64], P('tp'), may hold values from -0.75 to 0.75
- channel_decay_param: float32 [2048], P('tp'), may hold values from 3 to 10
- token_decay_offset: float32 [8192, 2048], P(('rep', 'fs'), 'tp'), may hold values from -0.7 to 0, as said below
- recurrent_output_weight: bfloat16 [2048, 2048], P('tp', 'fs'), may hold values from -0.125 to 0.125
- up_projection_weight: bfloat16 [2048, 6144], P('fs', 'tp'), may hold values from -0.125 to 0.125
- down_projection_weight: bfloat16 [6144, 2048], P('tp', 'fs'), may hold values from -0.078125 to 0.078125
Outputs:
- updated: bfloat16 [8192, 2048], P(('rep', 'fs'), 'tp')
Inputs may be any that keep to these rules, and one draw needn't show every extreme that they name: `token_decay_offset`: zero except at a few positions, where a whole row is negative.
All inputs are finite; a program needn't handle non-finite values.
Results may differ from a plain program's by a relative error of at most 0.015.
Values may be sent and summed in bfloat16 or wider, within the bound.
A program may use at most 128 MiB of HBM per device.

v0:
```python
import functools

import jax
import jax.numpy as jnp
from jax import lax
from jax.experimental import pallas as pl
from jax.experimental.pallas import tpu as pltpu
from jax.sharding import PartitionSpec as P


SEQ_LEN = 128
EPSILON = 1e-06
DECAY_MULTIPLIER = 8.0
LANES = 128


def half(values, which, axis):
    first, second = jnp.split(values, 2, axis)
    return jnp.where(which == 0, first, second)


def gather_shard(shard, ids, sizes):
    rep, fs, _ = ids
    _, n_fs, _ = sizes
    own, for_peer = shard
    hops = n_fs // 2
    place, side = fs // 2, fs % 2
    from_peer = lax.ppermute(for_peer, "fs", [(i, i ^ 1) for i in range(n_fs)])
    start = jnp.where(side == rep, own, from_peer)
    up = [(i, (i + 2) % n_fs) for i in range(n_fs)]
    down = [(i, (i + n_fs - 2) % n_fs) for i in range(n_fs)]
    pieces, places = [own, from_peer], [fs, fs ^ 1]
    below = above = start
    for step in range(1, hops):
        if step % 2:
            below = mine = lax.ppermute(below, "fs", up)
            base = 2 * ((place + hops - (step + 1) // 2) % hops)
        else:
            above = mine = lax.ppermute(above, "fs", down)
            base = 2 * ((place + step // 2) % hops)
        pieces += [mine, lax.ppermute(mine, "rep", [(0, 1), (1, 0)])]
        places += [base + rep, base + 1 - rep]
    return pieces, jnp.stack(places).astype(jnp.int32)


def gather_features(values, tp, n_tp):
    if n_tp != 2:
        return lax.all_gather(values, "tp", axis=1, tiled=True)
    other = lax.ppermute(values, "tp", [(0, 1), (1, 0)])
    return jnp.where(
        tp == 0, jnp.concatenate([values, other], 1), jnp.concatenate([other, values], 1)
    )


def sum_features(parts, tp, n_tp):
    total = lax.dynamic_index_in_dim(parts, tp, 0, False).astype(jnp.float32)
    for shift in range(1, n_tp):
        piece = lax.dynamic_index_in_dim(parts, (tp + shift) % n_tp, 0, False)
        got = lax.ppermute(piece, "tp", [(i, (i + shift) % n_tp) for i in range(n_tp)])
        total = total + got.astype(jnp.float32)
    return total.astype(jnp.bfloat16)


def norm_rows(values, gain):
    widened = values.astype(jnp.float32)
    inverse = lax.rsqrt(jnp.mean(widened * widened, axis=-1, keepdims=True) + EPSILON)
    return (widened * inverse * gain).astype(jnp.bfloat16)


ROWS = 256
CHUNK = 512


def depth_kernel(squared, places_ref, x_ref, *refs):
    *pieces, out_ref = refs
    depth, width = pieces[0].shape
    chunk = min(CHUNK, width)
    for lower in range(0, width, chunk):
        cols = slice(lower, lower + chunk)
        total = None
        for index, piece in enumerate(pieces):
            place = pl.multiple_of(places_ref[index] * depth, depth)
            term = jnp.dot(
                x_ref[:, pl.ds(place, depth)], piece[:, cols], preferred_element_type=jnp.float32
            )
            total = term if total is None else total + term
        if squared:
            total = jnp.square(jnp.maximum(total, 0.0))
        out_ref[:, cols] = total.astype(jnp.bfloat16)


def depth_matmul(x, gathered, squared=False):
    pieces, places = gathered
    tokens, width = x.shape
    shape = pieces[0].shape
    return pl.pallas_call(
        functools.partial(depth_kernel, squared),
        grid_spec=pltpu.PrefetchScalarGridSpec(
            num_scalar_prefetch=1,
            grid=(tokens // ROWS,),
            in_specs=[pl.BlockSpec((ROWS, width), lambda m, _: (m, 0))]
            + [pl.BlockSpec(shape, lambda m, _: (0, 0))] * len(pieces),
            out_specs=pl.BlockSpec((ROWS, shape[1]), lambda m, _: (m, 0)),
        ),
        out_shape=jax.ShapeDtypeStruct((tokens, shape[1]), jnp.bfloat16),
        cost_estimate=pl.CostEstimate(
            flops=2 * tokens * width * shape[1],
            bytes_accessed=2 * (tokens * width + (tokens + width) * shape[1]),
            transcendentals=0,
        ),
        name="depth_matmul",
    )(places, x, *pieces)


def columns_kernel(per, places_ref, x_ref, *refs):
    *pieces, out_ref = refs
    cols = pieces[0].shape[1]
    for index, piece in enumerate(pieces):
        place = places_ref[index]
        lower = pl.multiple_of((place % per) * cols, cols)
        out_ref[place // per, :, pl.ds(lower, cols)] = jnp.dot(
            x_ref[...], piece[...], preferred_element_type=jnp.float32
        ).astype(jnp.bfloat16)


def columns_matmul(x, gathered, n_tp, first, tokens):
    pieces, places = gathered
    depth, cols = pieces[0].shape
    per = len(pieces) // n_tp
    skip = first // ROWS
    return pl.pallas_call(
        functools.partial(columns_kernel, per),
        grid_spec=pltpu.PrefetchScalarGridSpec(
            num_scalar_prefetch=1,
            grid=(tokens // ROWS,),
            in_specs=[pl.BlockSpec((ROWS, depth), lambda m, _: (m + skip, 0))]
            + [pl.BlockSpec((depth, cols), lambda m, _: (0, 0))] * len(pieces),
            out_specs=pl.BlockSpec((n_tp, ROWS, per * cols), lambda m, _: (0, m, 0)),
        ),
        out_shape=jax.ShapeDtypeStruct((n_tp, tokens, per * cols), jnp.bfloat16),
        cost_estimate=pl.CostEstimate(
            flops=2 * tokens * depth * cols * len(pieces),
            bytes_accessed=2 * (tokens * depth + len(pieces) * cols * (depth + tokens)),
            transcendentals=0,
        ),
        name="columns_matmul",
    )(places, x, *pieces)


def shift_down(values, amount, fill):
    index = lax.broadcasted_iota(jnp.int32, values.shape, 0)
    return jnp.where(index < amount, fill, pltpu.roll(values, amount, 0))


def recurrence_kernel(
    side_ref, value_ref, gate_ref, own_ref, peer_ref, taps_ref, maps_ref, rate_ref, out_ref
):
    rows, channels = value_ref.shape
    reach = taps_ref.shape[0]
    per = LANES // maps_ref.shape[1]
    is_own = pl.program_id(0) < pl.num_programs(0) // 2
    for tile in range(channels // LANES):
        cols = slice(tile * LANES, (tile + 1) * LANES)
        values = value_ref[:, cols].astype(jnp.float32)
        filtered = taps_ref[reach - 1 : reach, cols] * values
        for back in range(1, reach):
            tap = taps_ref[reach - 1 - back : reach - back, cols]
            filtered = filtered + tap * shift_down(values, back, 0.0)
        conved = filtered.astype(jnp.bfloat16)
        maps = maps_ref[tile * per : (tile + 1) * per].reshape(LANES, 2 * LANES)
        logits = jnp.dot(conved, maps, preferred_element_type=jnp.float32)
        offset = jnp.where(is_own, own_ref[:, cols], peer_ref[:, cols].astype(jnp.float32))
        steps = 1.0 / (1.0 + jnp.exp(-logits))
        log_decay = steps[:, :LANES] * rate_ref[:, cols] + offset
        decay = jnp.exp(log_decay)
        y = -2.0 * log_decay
        series = 1.0 + y * (
            -1 / 2 + y * (1 / 6 + y * (-1 / 24 + y * (1 / 120 + y * (-1 / 720 + y * (1 / 5040)))))
        )
        lost = jnp.where(y < 0.35, y * series, 1.0 - decay * decay)
        state = jnp.sqrt(lost) * steps[:, LANES:] * conved.astype(jnp.float32)
        span = 1
        while span < rows:
            state = state + decay * shift_down(state, span, 0.0)
            if span * 2 < rows:
                decay = decay * shift_down(decay, span, 1.0)
            span *= 2
        gate = gate_ref[:, cols].astype(jnp.float32)
        gelu = 0.5 * gate * (1.0 + lax.erf(gate * 0.7071067811865476))
        out_ref[:, cols] = (state * gelu).astype(jnp.bfloat16)


def recurrence(projected, offset_own, offset_peer, taps, decay_maps, input_maps, rate, side):
    tokens = projected.shape[0]
    channels = offset_peer.shape[1]
    blocks, size, _ = decay_maps.shape
    per = LANES // size
    block = jnp.arange(blocks)[:, None, None] % per
    group = jnp.arange(LANES)[None, None, :] // size

    def diagonal(maps):
        return jnp.where(block == group, jnp.tile(maps, (1, 1, per)), 0)

    maps = jnp.concatenate([diagonal(decay_maps), diagonal(input_maps)], 2)
    sequences = tokens // SEQ_LEN
    own = sequences // 2
    return pl.pallas_call(
        recurrence_kernel,
        grid_spec=pltpu.PrefetchScalarGridSpec(
            num_scalar_prefetch=1,
            grid=(sequences,),
            in_specs=[
                pl.BlockSpec((SEQ_LEN, channels), lambda s, side: (s, 0)),
                pl.BlockSpec((SEQ_LEN, channels), lambda s, side: (s, 1)),
                pl.BlockSpec(
                    (SEQ_LEN, channels), lambda s, side: (jnp.minimum(s, own - 1), side[0])
                ),
                pl.BlockSpec((SEQ_LEN, channels), lambda s, side: (jnp.maximum(s - own, 0), 0)),
                pl.BlockSpec((taps.shape[0], channels), lambda s, side: (0, side[0])),
                pl.BlockSpec((blocks // 2, size, 2 * LANES), lambda s, side: (side[0], 0, 0)),
                pl.BlockSpec((1, channels), lambda s, side: (0, side[0])),
            ],
            out_specs=pl.BlockSpec((SEQ_LEN, channels), lambda s, side: (s, 0)),
        ),
        out_shape=jax.ShapeDtypeStruct((tokens, channels), jnp.bfloat16),
        cost_estimate=pl.CostEstimate(
            flops=tokens * channels * 700,
            bytes_accessed=tokens * channels * 10,
            transcendentals=tokens * channels * 6,
        ),
        name="recurrence",
    )(
        side.astype(jnp.int32)[None],
        projected,
        projected,
        offset_own,
        offset_peer,
        taps.astype(jnp.float32),
        maps,
        rate[None, :],
    )


def shards(
    sizes,
    stream,
    recurrent_norm_gain,
    feedforward_norm_gain,
    recurrent_input_weight,
    output_gate_weight,
    causal_filter_weight,
    decay_gate_matrix,
    input_gate_matrix,
    channel_decay_param,
    token_decay_offset,
    recurrent_output_weight,
    up_projection_weight,
    down_projection_weight,
):
    _, n_fs, n_tp = sizes
    ids = lax.axis_index("rep"), lax.axis_index("fs"), lax.axis_index("tp")
    _, fs, tp = ids
    side = fs % 2
    pairs = [(i, i ^ 1) for i in range(n_fs)]
    tokens = stream.shape[0]

    def halves(weight, axis):
        return half(weight, side, axis), half(weight, 1 - side, axis)

    def to_peer(values):
        return lax.ppermute(values, "fs", pairs)

    value_own, value_peer = halves(recurrent_input_weight, 1)
    gate_own, gate_peer = halves(output_gate_weight, 1)
    entry = (
        jnp.concatenate([value_own, gate_own], 1),
        jnp.concatenate([value_peer, gate_peer], 1),
    )
    entry_full = gather_shard(entry, ids, sizes)
    stream_peer = to_peer(stream)
    offset_peer = to_peer(half(token_decay_offset, 1 - side, 1).astype(jnp.bfloat16))
    output_full = gather_shard(halves(recurrent_output_weight, 0), ids, sizes)
    expand_full = gather_shard(halves(up_projection_weight, 1), ids, sizes)
    contract_full = gather_shard(halves(down_projection_weight, 0), ids, sizes)

    own_pair = jnp.concatenate([stream, stream_peer], 0)
    whole = gather_features(own_pair, tp, n_tp)
    normed = norm_rows(whole, recurrent_norm_gain)
    projected = depth_matmul(normed, entry_full)
    mixed = recurrence(
        projected,
        token_decay_offset,
        offset_peer,
        causal_filter_weight,
        decay_gate_matrix,
        input_gate_matrix,
        -DECAY_MULTIPLIER * jax.nn.softplus(-channel_decay_param),
        side,
    )
    mixer_terms = columns_matmul(mixed, output_full, n_tp, 0, 2 * tokens)
    mixer_chip = sum_features(mixer_terms, tp, n_tp)
    got_own = to_peer(mixer_chip[tokens:])
    got_peer = to_peer(mixer_chip[:tokens])
    update = mixer_chip.astype(jnp.float32) + jnp.concatenate([got_own, got_peer], 0).astype(
        jnp.float32
    )
    middle = (own_pair.astype(jnp.float32) + update).astype(jnp.bfloat16)
    normed_mid = norm_rows(gather_features(middle, tp, n_tp), feedforward_norm_gain)
    activity = depth_matmul(normed_mid, expand_full, squared=True)
    peer_terms = columns_matmul(activity, contract_full, n_tp, tokens, tokens)
    got = to_peer(sum_features(peer_terms, tp, n_tp))
    own_terms = columns_matmul(activity, contract_full, n_tp, 0, tokens)
    own_chip = sum_features(own_terms, tp, n_tp)
    channel_sum = own_chip.astype(jnp.float32) + got.astype(jnp.float32)
    return (middle[:tokens].astype(jnp.float32) + channel_sum).astype(jnp.bfloat16)


MESH = pl.DeviceIdType.MESH
CHUNK_ROWS = 128


def whole_kernel(
    stream_ref,
    offset_ref,
    first_gain_ref,
    second_gain_ref,
    taps_ref,
    decay_maps_ref,
    input_maps_ref,
    rate_ref,
    value_hbm,
    gate_hbm,
    output_hbm,
    raise_hbm,
    lower_hbm,
    out_ref,
    weights,
    normed,
    normed_mid,
    square_own,
    square_got,
    projected,
    mixed,
    offsets,
    offset_send,
    maps,
    kept,
    passed,
    got,
    mid_send,
    mid_got,
    middle,
    activity,
    partial,
    partial_got,
    last_send,
    last_got,
    local_sem,
    y_send,
    y_recv,
    z_send,
    z_recv,
    x_send,
    x_recv,
    act_send,
    act_recv,
):
    rep, fs, tp = lax.axis_index("rep"), lax.axis_index("fs"), lax.axis_index("tp")
    z, y = fs // 2, fs % 2
    tokens, half_width = stream_ref.shape
    width = 2 * half_width
    chunks, _, n_fs, block, _ = weights.shape
    quarter = half_width // 2
    lane_tiles = half_width // LANES
    raises = (chunks - 3) // 2
    is_mid = jnp.logical_or(z == 1, z == 2)
    low = (z // 2) == tp

    def plane(m):
        return 2 * ((z // 2 + m // 2) % 2) + (z % 2 + m % 2) % 2

    x_peer = (1 - rep, fs, tp)
    y_peer = (rep, 2 * z + 1 - y, tp)
    t_peer = (rep, fs, 1 - tp)

    def z_peer(m):
        return (rep, 2 * plane(m) + y, tp)

    barrier = pltpu.get_barrier_semaphore()
    for peer in (x_peer, y_peer, t_peer, z_peer(1), z_peer(2), z_peer(3)):
        pl.semaphore_signal(barrier, inc=1, device_id=peer, device_id_type=MESH)
    pl.semaphore_wait(barrier, 6)

    def remote(src, dst, send, recv, peer):
        return pltpu.make_async_remote_copy(
            src_ref=src, dst_ref=dst, send_sem=send, recv_sem=recv, device_id=peer, device_id_type=MESH
        )

    def shard_block(k, side, part):
        if k < 2 or 3 <= k < 3 + raises:
            ref = (value_hbm, gate_hbm)[k] if k < 2 else raise_hbm
            first = 0 if k < 2 else (k - 3) * quarter
            span = ref.shape[1] // 2
            start = pl.multiple_of(side * span + first + part * block, block)
            return ref.at[:, pl.ds(start, block)]
        ref = output_hbm if k == 2 else lower_hbm
        first = 0 if k == 2 else (k - 3 - raises) * quarter
        span = ref.shape[0] // 2
        start = pl.multiple_of(side * span + first + part * block, block)
        return ref.at[pl.ds(start, block), :]

    def part_of(q):
        return rep if q == 0 else 1 - rep

    def local_copy(k, q):
        part = part_of(q)
        return pltpu.make_async_copy(
            shard_block(k, y, part), weights.at[k, part, fs], local_sem.at[k, q]
        )

    def y_copy(k, q):
        part = part_of(q)
        return remote(
            shard_block(k, 1 - y, part), weights.at[k, part, fs], y_send.at[k, q], y_recv.at[k, q], y_peer
        )

    def z_copy(k, h, m):
        spot = weights.at[k, rep, fs if h == 0 else 2 * z + 1 - y]
        src = shard_block(k, y, rep) if h == 0 else spot
        return remote(src, spot, z_send.at[k, h, m - 1], z_recv.at[k, h, m - 1], z_peer(m))

    def z_relay(k, h):
        spot = weights.at[k, rep, 2 * plane(2) + (y if h == 0 else 1 - y)]
        return remote(spot, spot, z_send.at[k, h, 3], z_recv.at[k, h, 2], z_peer(1))

    def x_copy(k, h, m):
        spot = weights.at[k, rep, 2 * plane(m) + (y if h == 0 else 1 - y)]
        return remote(spot, spot, x_send.at[k, h, m - 1], x_recv.at[k, h, m - 1], x_peer)

    def z_start(k, h):
        z_copy(k, h, 2).start()
        z_copy(k, h, 1).start()

        @pl.when(is_mid)
        def _():
            z_copy(k, h, 3).start()

    def forward_y(k):
        y_copy(k, 0).wait_recv()
        z_start(k, 1)

    def relay(k, h, m):
        z_copy(k, h, m).wait_recv()
        x_copy(k, h, m).start()

        @pl.when(jnp.logical_and(is_mid, m == 2))
        def _():
            z_relay(k, h).start()

    def relay_all(k, h):
        for m in (1, 2, 3):
            relay(k, h, m)

    def relay_at(index, k, h):
        @pl.when(index < 3)
        def _():
            relay(k, h, index + 1)

    def wait_own(k):
        for q in range(2):
            local_copy(k, q).wait()
        y_copy(k, 1).wait_recv()

    def wait_x(k, h):
        for m in (1, 2, 3):
            x_copy(k, h, m).wait_recv()

    def tp_copy(src, dst, slot):
        return remote(src, dst, act_send.at[slot], act_recv.at[slot], t_peer)

    def y_act(src, dst, slot):
        return remote(src, dst, act_send.at[slot], act_recv.at[slot], y_peer)

    for k in range(3):
        for q in range(2):
            y_copy(k, q).start()
    for k in range(2):
        z_start(k, 0)
    for k in range(chunks):
        for q in range(2):
            local_copy(k, q).start()

    own_columns = pl.ds(pl.multiple_of(tp * half_width, half_width), half_width)

    def squares(source, phase):
        def body(step, _):
            rows = pl.ds(pl.multiple_of(step * CHUNK_ROWS, CHUNK_ROWS), CHUNK_ROWS)
            total = None
            for tile in range(lane_tiles):
                value = source[rows, tile * LANES : (tile + 1) * LANES].astype(jnp.float32)
                total = value * value if total is None else total + value * value
            square_own[phase, rows, :] = total
            return 0

        lax.fori_loop(0, tokens // CHUNK_ROWS, body, 0)

    def square_copy(phase):
        return tp_copy(square_own.at[phase], square_got.at[phase], 9 + phase)

    def norm(source, phase, gain_ref, target):
        def body(step, _):
            rows = pl.ds(pl.multiple_of(step * CHUNK_ROWS, CHUNK_ROWS), CHUNK_ROWS)
            total = jnp.sum(square_own[phase, rows, :] + square_got[phase, rows, :], axis=1, keepdims=True)
            inverse = lax.rsqrt(total * (1.0 / width) + EPSILON)
            for tile in range(lane_tiles):
                value = source[rows, tile * LANES : (tile + 1) * LANES].astype(jnp.float32)
                gain = gain_ref[pl.ds(tp * lane_tiles + tile, 1), :]
                lanes = pl.ds(pl.multiple_of(tp * half_width + tile * LANES, LANES), LANES)
                target[y, rows, lanes] = (value * inverse * gain).astype(jnp.bfloat16)
            return 0

        lax.fori_loop(0, tokens // CHUNK_ROWS, body, 0)

    def block_copies(target, base):
        own = target.at[y, :, own_columns]
        theirs = target.at[1 - y, :, own_columns]
        return (
            tp_copy(own, own, base),
            y_act(own, own, base + 1),
            tp_copy(theirs, theirs, base + 2),
        )

    squares(stream_ref, 0)
    square_copy(0).start()
    mine = pl.ds(pl.multiple_of(y * quarter, quarter), quarter)
    peers = pl.ds(pl.multiple_of((1 - y) * quarter, quarter), quarter)
    offset_send[...] = offset_ref[:, peers].astype(jnp.bfloat16)
    offsets[0] = offset_ref[:, mine].astype(jnp.bfloat16)
    square_copy(0).wait_recv()
    norm(stream_ref, 0, first_gain_ref, normed)
    first_tp, first_y, first_pass = block_copies(normed, 0)
    first_y.start()
    first_tp.start()
    offset_copy = y_act(offset_send, offsets.at[1], 3)
    offset_copy.start()
    for k in range(3, 3 + raises):
        for q in range(2):
            y_copy(k, q).start()

    forward_y(0)
    relay_all(0, 0)
    forward_y(1)
    z_start(2, 0)
    relay_all(0, 1)
    forward_y(2)
    for k in range(3, 3 + raises):
        z_start(k, 0)
    relay_all(1, 0)

    size = decay_maps_ref.shape[1]
    per = LANES // size
    tiles = quarter // LANES
    maps[...] = jnp.zeros_like(maps)
    for tile in range(tiles):
        for index in range(per):
            place = y * (tiles * per) + tile * per + index
            span = slice(index * size, (index + 1) * size)
            maps[tile, span, index * size : (index + 1) * size] = decay_maps_ref[place]
            maps[tile, span, LANES + index * size : LANES + (index + 1) * size] = input_maps_ref[place]

    relay_all(1, 1)
    first_y.wait_recv()
    first_pass.start()

    for k in range(2):
        wait_own(k)
    for k in range(2):
        for h in range(2):
            wait_x(k, h)
    first_tp.wait_recv()

    def project(which, token_block, relays):
        def body(step, _):
            relay_at(step, *relays)
            matrix = weights[step // 2, step % 2].reshape(width, block)
            projected[which, step] = jnp.dot(
                normed[token_block], matrix, preferred_element_type=jnp.float32
            ).astype(jnp.bfloat16)
            return 0

        lax.fori_loop(0, 4, body, 0)

    reach = taps_ref.shape[0]

    def recur(which, relays):
        def body(step, _):
            relay_at(step, *relays)
            rows = pl.ds(pl.multiple_of(step * SEQ_LEN, SEQ_LEN), SEQ_LEN)
            for tile in range(tiles):
                part, lane = tile * LANES // block, tile * LANES % block
                lanes = slice(lane, lane + LANES)
                taps = taps_ref[
                    :, pl.ds(pl.multiple_of(y * quarter + tile * LANES, LANES), LANES)
                ].astype(jnp.float32)
                values = projected[which, part, rows, lanes].astype(jnp.float32)
                filtered = taps[reach - 1 : reach] * values
                for back in range(1, reach):
                    tap = taps[reach - 1 - back : reach - back]
                    filtered = filtered + tap * shift_down(values, back, 0.0)
                conved = filtered.astype(jnp.bfloat16)
                logits = jnp.dot(conved, maps[tile], preferred_element_type=jnp.float32)
                offset = offsets[which, rows, tile * LANES : (tile + 1) * LANES].astype(jnp.float32)
                steps = 1.0 / (1.0 + jnp.exp(-logits))
                rate = rate_ref[pl.ds(y * tiles + tile, 1), :]
                log_decay = steps[:, :LANES] * rate + offset
                decay = jnp.exp(log_decay)
                twice = -2.0 * log_decay
                series = 1.0 + twice * (
                    -1 / 2
                    + twice
                    * (1 / 6 + twice * (-1 / 24 + twice * (1 / 120 + twice * (-1 / 720 + twice * (1 / 5040)))))
                )
                lost = jnp.where(twice < 0.35, twice * series, 1.0 - decay * decay)
                state = jnp.sqrt(lost) * steps[:, LANES:] * conved.astype(jnp.float32)
                span = 1
                while span < SEQ_LEN:
                    state = state + decay * shift_down(state, span, 0.0)
                    if span * 2 < SEQ_LEN:
                        decay = decay * shift_down(decay, span, 1.0)
                    span *= 2
                gate = projected[which, 2 + part, rows, lanes].astype(jnp.float32)
                gelu = 0.5 * gate * (1.0 + lax.erf(gate * 0.7071067811865476))
                mixed[which, rows, tile * LANES : (tile + 1) * LANES] = (state * gelu).astype(jnp.bfloat16)
            return 0

        lax.fori_loop(0, tokens // SEQ_LEN, body, 0)

    project(0, y, (2, 0))
    recur(0, (2, 1))
    first_pass.wait_recv()
    project(1, 1 - y, (3, 0))
    offset_copy.wait_recv()
    recur(1, (4, 0))

    wait_own(2)
    wait_x(2, 0)
    wait_x(2, 1)

    def mix_out(which):
        def body(step, _):
            def term(place):
                matrix = weights[2, :, place].reshape(quarter, block)
                return jnp.dot(mixed[which], matrix, preferred_element_type=jnp.float32).astype(jnp.bfloat16)

            lanes = pl.ds(pl.multiple_of(step * block, block), block)
            per_half = n_fs // 2
            passed[which, :, lanes] = term(per_half * (1 - tp) + step)
            kept[which, :, lanes] = term(per_half * tp + step)
            return 0

        lax.fori_loop(0, n_fs // 2, body, 0)

    def mix_copy(which):
        return tp_copy(passed.at[which], got.at[which], 4 + which)

    mix_out(1)
    mix_copy(1).start()
    mix_out(0)
    mix_copy(0).start()

    def add_peer(step, _):
        rows = pl.ds(pl.multiple_of(step * CHUNK_ROWS, CHUNK_ROWS), CHUNK_ROWS)
        mid_send[rows, :] = (
            kept[1, rows, :].astype(jnp.float32) + got[1, rows, :].astype(jnp.float32)
        ).astype(jnp.bfloat16)
        return 0

    mix_copy(1).wait_recv()
    lax.fori_loop(0, tokens // CHUNK_ROWS, add_peer, 0)
    mid_copy = y_act(mid_send, mid_got, 6)
    mid_copy.start()

    last_raise = 3 + raises
    for k in range(5, last_raise):
        relay_all(k, 0)
    for k in range(3, last_raise):
        forward_y(k)
    for k in range(last_raise, chunks):
        z_start(k, 0)
    mix_copy(0).wait_recv()
    relay_all(3, 1)

    mid_copy.wait_recv()

    def add_own(step, _):
        rows = pl.ds(pl.multiple_of(step * CHUNK_ROWS, CHUNK_ROWS), CHUNK_ROWS)
        total = None
        for tile in range(lane_tiles):
            lanes = slice(tile * LANES, (tile + 1) * LANES)
            update = kept[0, rows, lanes].astype(jnp.float32) + got[0, rows, lanes].astype(jnp.float32)
            update = update + mid_got[rows, lanes].astype(jnp.float32)
            value = (stream_ref[rows, lanes].astype(jnp.float32) + update).astype(jnp.bfloat16)
            middle[rows, lanes] = value
            value = value.astype(jnp.float32)
            total = value * value if total is None else total + value * value
        square_own[1, rows, :] = total
        return 0

    lax.fori_loop(0, tokens // CHUNK_ROWS, add_own, 0)
    square_copy(1).start()
    square_copy(1).wait_recv()
    norm(middle, 1, second_gain_ref, normed_mid)
    second_tp, second_y, second_pass = block_copies(normed_mid, 11)
    second_y.start()
    second_tp.start()
    for k in range(last_raise, chunks):
        for q in range(2):
            y_copy(k, q).start()

    for k in range(4, last_raise):
        relay_all(k, 1)
    for k in range(3, last_raise):
        wait_own(k)
        wait_x(k, 0)
        wait_x(k, 1)

    def lift(which, token_block, relays):
        def body(step, _):
            relay_at(step, *relays)
            matrix = weights[3 + step // 2, step % 2].reshape(width, block)
            total = jnp.dot(normed_mid[token_block], matrix, preferred_element_type=jnp.float32)
            lanes = pl.ds(pl.multiple_of(step * block, block), block)
            activity[which, :, lanes] = jnp.square(jnp.maximum(total, 0.0)).astype(jnp.bfloat16)
            return 0

        lax.fori_loop(0, 2 * raises, body, 0)

    second_tp.wait_recv()
    lift(0, y, (last_raise, 0))
    second_y.wait_recv()
    second_pass.start()
    second_pass.wait_recv()
    lift(1, 1 - y, (last_raise + 1, 0))
    for k in range(last_raise + 2, chunks):
        relay_all(k, 0)
    for k in range(last_raise, chunks):
        forward_y(k)

    depth = raises * quarter

    def lower(h, m):
        place = 2 * plane(m) + (y if h == 0 else 1 - y)

        def body(which, _):
            matrix = weights[last_raise:chunks, :, place].reshape(depth, block)
            partial[m, h, which] = jnp.dot(
                activity[which], matrix, preferred_element_type=jnp.float32
            ).astype(jnp.bfloat16)
            return 0

        lax.fori_loop(0, 2, body, 0)

    def is_owner(m):
        return low if m < 2 else jnp.logical_not(low)

    def owner_copy(h, m):
        slot = 14 + 2 * (m % 2) + h
        return tp_copy(partial.at[m, h], partial_got.at[m % 2, h], slot)

    def last_copy(h, m):
        slot = 18 + 2 * (m % 2)
        return remote(
            last_send.at[m % 2, h],
            last_got.at[m % 2, 1 - h],
            act_send.at[slot + h],
            act_recv.at[slot + 1 - h],
            y_peer,
        )

    def pass_on(h, m):
        @pl.when(jnp.logical_not(is_owner(m)))
        def _():
            owner_copy(h, m).start()

    def finish(h, m):
        @pl.when(is_owner(m))
        def _():
            owner_copy(h, m).wait_recv()

            def body(step, _):
                rows = pl.ds(pl.multiple_of(step * CHUNK_ROWS, CHUNK_ROWS), CHUNK_ROWS)
                last_send[m % 2, h, rows, :] = (
                    partial[m, h, 1, rows, :].astype(jnp.float32)
                    + partial_got[m % 2, h, 1, rows, :].astype(jnp.float32)
                ).astype(jnp.bfloat16)
                return 0

            lax.fori_loop(0, tokens // CHUNK_ROWS, body, 0)
            last_copy(h, m).start()

    def close(h, mm):
        owned = mm + 2 * (1 - low.astype(jnp.int32))
        last_copy(1 - h, mm).wait_recv()
        place = 2 * ((z % 2 + mm) % 2) + (y if h == 0 else 1 - y)
        lanes = pl.ds(pl.multiple_of(place * block, block), block)

        def body(step, _):
            rows = pl.ds(pl.multiple_of(step * CHUNK_ROWS, CHUNK_ROWS), CHUNK_ROWS)
            update = (
                partial[owned, h, 0, rows, :].astype(jnp.float32)
                + partial_got[mm, h, 0, rows, :].astype(jnp.float32)
                + last_got[mm, h, rows, :].astype(jnp.float32)
            )
            out_ref[rows, lanes] = (middle[rows, lanes].astype(jnp.float32) + update).astype(jnp.bfloat16)
            return 0

        lax.fori_loop(0, tokens // CHUNK_ROWS, body, 0)

    for k in range(last_raise, chunks):
        wait_own(k)
        wait_x(k, 0)
    order = [(0, m) for m in range(4)] + [(1, m) for m in range(4)]
    for index, (h, m) in enumerate(order):
        if index == 5:
            for k in range(last_raise, chunks):
                relay_all(k, 1)
            for k in range(last_raise, chunks):
                wait_x(k, 1)
        lower(h, m)
        pass_on(h, m)
        if index:
            finish(*order[index - 1])
    finish(*order[-1])
    for h in range(2):
        for mm in range(2):
            close(h, mm)

    for k in range(chunks):
        for q in range(2):
            y_copy(k, q).wait_send()
        for h in range(2):
            z_copy(k, h, 1).wait_send()
            z_copy(k, h, 2).wait_send()

            @pl.when(is_mid)
            def _():
                z_copy(k, h, 3).wait_send()
                z_relay(k, h).wait_send()

            for m in (1, 2, 3):
                x_copy(k, h, m).wait_send()
    for copy in (first_tp, first_y, first_pass, second_tp, second_y, second_pass, offset_copy, mid_copy):
        copy.wait_send()
    for phase in range(2):
        square_copy(phase).wait_send()
        mix_copy(phase).wait_send()
    for h, m in order:

        @pl.when(is_owner(m))
        def _():
            last_copy(h, m).wait_send()

        @pl.when(jnp.logical_not(is_owner(m)))
        def _():
            owner_copy(h, m).wait_send()


def whole_layer(
    stream,
    recurrent_norm_gain,
    feedforward_norm_gain,
    recurrent_input_weight,
    output_gate_weight,
    causal_filter_weight,
    decay_gate_matrix,
    input_gate_matrix,
    channel_decay_param,
    token_decay_offset,
    recurrent_output_weight,
    up_projection_weight,
    down_projection_weight,
):
    tokens, half_width = stream.shape
    width = 2 * half_width
    quarter = half_width // 2
    block, n_fs = quarter // 2, 8
    raises = up_projection_weight.shape[1] // half_width
    chunks = 3 + 2 * raises
    depth = raises * quarter
    tiles = quarter // LANES
    half_type, full_type = jnp.bfloat16, jnp.float32
    rate = -DECAY_MULTIPLIER * jax.nn.softplus(-channel_decay_param)
    vmem = pl.BlockSpec(memory_space=pltpu.VMEM)
    anywhere = pl.BlockSpec(memory_space=pl.ANY)
    dma = pltpu.SemaphoreType.DMA
    return pl.pallas_call(
        whole_kernel,
        out_shape=jax.ShapeDtypeStruct((tokens, half_width), half_type),
        in_specs=[vmem] * 8 + [anywhere] * 5,
        out_specs=vmem,
        scratch_shapes=[
            pltpu.VMEM((chunks, 2, n_fs, block, block), half_type),
            pltpu.VMEM((2, tokens, width), half_type),
            pltpu.VMEM((2, tokens, width), half_type),
            pltpu.VMEM((2, tokens, LANES), full_type),
            pltpu.VMEM((2, tokens, LANES), full_type),
            pltpu.VMEM((2, 4, tokens, block), half_type),
            pltpu.VMEM((2, tokens, quarter), half_type),
            pltpu.VMEM((2, tokens, quarter), half_type),
            pltpu.VMEM((tokens, quarter), half_type),
            pltpu.VMEM((tiles, LANES, 2 * LANES), half_type),
            pltpu.VMEM((2, tokens, half_width), half_type),
            pltpu.VMEM((2, tokens, half_width), half_type),
            pltpu.VMEM((2, tokens, half_width), half_type),
            pltpu.VMEM((tokens, half_width), half_type),
            pltpu.VMEM((tokens, half_width), half_type),
            pltpu.VMEM((tokens, half_width), half_type),
            pltpu.VMEM((2, tokens, depth), half_type),
            pltpu.VMEM((4, 2, 2, tokens, block), half_type),
            pltpu.VMEM((2, 2, 2, tokens, block), half_type),
            pltpu.VMEM((2, 2, tokens, block), half_type),
            pltpu.VMEM((2, 2, tokens, block), half_type),
            dma((chunks, 2)),
            dma((chunks, 2)),
            dma((chunks, 2)),
            dma((chunks, 2, 4)),
            dma((chunks, 2, 3)),
            dma((chunks, 2, 3)),
            dma((chunks, 2, 3)),
            dma((22,)),
            dma((22,)),
        ],
        compiler_params=pltpu.CompilerParams(
            collective_id=0, has_side_effects=True, vmem_limit_bytes=67043328
        ),
        name="whole_layer",
    )(
        stream,
        token_decay_offset,
        recurrent_norm_gain.reshape(-1, LANES),
        feedforward_norm_gain.reshape(-1, LANES),
        causal_filter_weight,
        decay_gate_matrix,
        input_gate_matrix,
        rate.reshape(-1, LANES),
        recurrent_input_weight,
        output_gate_weight,
        recurrent_output_weight,
        up_projection_weight,
        down_projection_weight,
    )


def fits_whole(sizes, stream, up_projection_weight, decay_gate_matrix):
    tokens, half_width = stream.shape
    return (
        sizes == (2, 8, 2)
        and half_width % (8 * LANES) == 0
        and tokens % (4 * SEQ_LEN) == 0
        and up_projection_weight.shape[1] % half_width == 0
        and up_projection_weight.shape[1] // half_width >= 2
        and LANES % decay_gate_matrix.shape[1] == 0
    )


def solution(mesh):
    in_specs = (
        P(("rep", "fs"), "tp"),
        P(),
        P(),
        P("fs", "tp"),
        P("fs", "tp"),
        P(None, "tp"),
        P("tp", None, None),
        P("tp", None, None),
        P("tp"),
        P(("rep", "fs"), "tp"),
        P("tp", "fs"),
        P("fs", "tp"),
        P("tp", "fs"),
    )
    out_specs = P(("rep", "fs"), "tp")
    sizes = tuple(mesh.shape[axis] for axis in ("rep", "fs", "tp"))

    def body(*args):
        if fits_whole(sizes, args[0], args[11], args[6]):
            return whole_layer(*args)
        return shards(sizes, *args)

    return jax.shard_map(
        body, mesh=mesh, in_specs=in_specs, out_specs=out_specs, check_vma=False
    )
```

profile of v0, /device:TPU:0, one launch (start us, length us, event | category | flops | bytes accessed | tf_op | source)
XLA Modules:
  0.0 229.6 jit_solution(7247982466340568974)
XLA Ops:
  0.0 1.3 fusion.1.rate_ref
  1.3 226.0 %whole_layer.1 = bf16[512,1024]{1,0:T(8,128)(2,1)} custom-call(bf16[512,1024]{1,0:T(8,128)(2,1)} %stream_ref.1, f32[512,1024]{1,0:T(8,128)} %offset_ref.1, f32[16,128]{1,0:T(8,128)} %bitcast.4, f32[16,128]{1,0:T(8,128)} %bitcast.5, bf16[4,1024]{1,0:T(4,128)(2,1)} %taps_ref.1, bf16[16,64,64]{2,1,0:T(8,128)(2,1)} %decay_maps_ref.1, ...), custom_call_target="tpu_custom_call" | custom-call | tf_op jit(solution)/shard_map/whole_layer/pallas_call | solution.py:896
  227.3 2.3 copy.15
where the time goes:
time: 232 us; the launch traced here: 230 us
  Pallas kernels  226 us (97%)
    pallas_call x1, Pallas kernels, whole_layer(): pl.pallas_call(whole_kernel, out_shape=jax.ShapeDtypeStruct((tokens, half...  226 us

commit v1 on v0

--- a/solution.py
+++ b/solution.py
@@ -317,23 +317,27 @@
 
 MESH = pl.DeviceIdType.MESH
 CHUNK_ROWS = 128
+AHEAD = (2, 2, 2, 3)
 
 
 def whole_kernel(
-    stream_ref,
-    offset_ref,
+    stream_hbm,
+    offset_hbm,
     first_gain_ref,
     second_gain_ref,
     taps_ref,
     decay_maps_ref,
     input_maps_ref,
-    rate_ref,
+    param_ref,
     value_hbm,
     gate_hbm,
     output_hbm,
     raise_hbm,
     lower_hbm,
     out_ref,
+    stream_ref,
+    offset_ref,
+    rate_ref,
     weights,
     normed,
     normed_mid,
@@ -364,6 +368,7 @@
     x_recv,
     act_send,
     act_recv,
+    load_sem,
 ):
     rep, fs, tp = lax.axis_index("rep"), lax.axis_index("fs"), lax.axis_index("tp")
     z, y = fs // 2, fs % 2
@@ -385,6 +390,13 @@
 
     def z_peer(m):
         return (rep, 2 * plane(m) + y, tp)
+
+    loads = (
+        pltpu.make_async_copy(stream_hbm, stream_ref, load_sem.at[0]),
+        pltpu.make_async_copy(offset_hbm, offset_ref, load_sem.at[1]),
+    )
+    for load in loads:
+        load.start()
 
     barrier = pltpu.get_barrier_semaphore()
     for peer in (x_peer, y_peer, t_peer, z_peer(1), z_peer(2), z_peer(3)):
@@ -437,17 +449,35 @@
         spot = weights.at[k, rep, 2 * plane(m) + (y if h == 0 else 1 - y)]
         return remote(spot, spot, x_send.at[k, h, m - 1], x_recv.at[k, h, m - 1], x_peer)
 
-    def z_start(k, h):
-        z_copy(k, h, 2).start()
-        z_copy(k, h, 1).start()
-
-        @pl.when(is_mid)
-        def _():
-            z_copy(k, h, 3).start()
-
-    def forward_y(k):
-        y_copy(k, 0).wait_recv()
-        z_start(k, 1)
+    last_raise = 3 + raises
+    lowers = range(last_raise, chunks)
+    every = (2, 1, 3)
+    events = [(k, h, every) for k, h in ((0, 0), (1, 0), (0, 1), (1, 1), (2, 0), (2, 1))]
+    events += [(k, h, every) for h in range(2) for k in range(3, last_raise)]
+    events += [(k, 0, every) for k in lowers]
+    events += [(k, 1, (2, 3)) for k in lowers] + [(k, 1, (1,)) for k in lowers]
+
+    def reach_of(index):
+        return index + AHEAD[min(index, len(AHEAD) - 1)]
+
+    def start_after(index):
+        for later in range(reach_of(index - 1) + 1 if index else 2, reach_of(index) + 1):
+            start(later)
+
+    def start(index):
+        if index >= len(events):
+            return
+        k, h, sources = events[index]
+        if h == 1 and 2 in sources:
+            y_copy(k, 0).wait_recv()
+        for m in sources:
+            if m < 3:
+                z_copy(k, h, m).start()
+            else:
+
+                @pl.when(is_mid)
+                def _():
+                    z_copy(k, h, 3).start()
 
     def relay(k, h, m):
         z_copy(k, h, m).wait_recv()
@@ -457,14 +487,23 @@
         def _():
             z_relay(k, h).start()
 
-    def relay_all(k, h):
-        for m in (1, 2, 3):
+    def advance(index):
+        k, h, sources = events[index]
+        for place, m in enumerate(sorted(sources)):
             relay(k, h, m)
-
-    def relay_at(index, k, h):
-        @pl.when(index < 3)
+            if place == 0:
+                start_after(index)
+
+    def advance_at(step, index):
+        k, h, _ = events[index]
+
+        @pl.when(step < 3)
         def _():
-            relay(k, h, index + 1)
+            relay(k, h, step + 1)
+
+        @pl.when(step == 0)
+        def _():
+            start_after(index)
 
     def wait_own(k):
         for q in range(2):
@@ -481,11 +520,13 @@
     def y_act(src, dst, slot):
         return remote(src, dst, act_send.at[slot], act_recv.at[slot], y_peer)
 
-    for k in range(3):
+    def y_start(k):
         for q in range(2):
             y_copy(k, q).start()
-    for k in range(2):
-        z_start(k, 0)
+
+    y_start(0)
+    y_start(1)
+    start(0)
     for k in range(chunks):
         for q in range(2):
             local_copy(k, q).start()
@@ -530,8 +571,10 @@
             tp_copy(theirs, theirs, base + 2),
         )
 
+    loads[0].wait()
     squares(stream_ref, 0)
     square_copy(0).start()
+    loads[1].wait()
     mine = pl.ds(pl.multiple_of(y * quarter, quarter), quarter)
     peers = pl.ds(pl.multiple_of((1 - y) * quarter, quarter), quarter)
     offset_send[...] = offset_ref[:, peers].astype(jnp.bfloat16)
@@ -539,23 +582,23 @@
     square_copy(0).wait_recv()
     norm(stream_ref, 0, first_gain_ref, normed)
     first_tp, first_y, first_pass = block_copies(normed, 0)
-    first_y.start()
     first_tp.start()
     offset_copy = y_act(offset_send, offsets.at[1], 3)
+
+    y_start(2)
+    start(1)
+    advance(0)
+    first_y.start()
+    advance(1)
     offset_copy.start()
-    for k in range(3, 3 + raises):
-        for q in range(2):
-            y_copy(k, q).start()
-
-    forward_y(0)
-    relay_all(0, 0)
-    forward_y(1)
-    z_start(2, 0)
-    relay_all(0, 1)
-    forward_y(2)
-    for k in range(3, 3 + raises):
-        z_start(k, 0)
-    relay_all(1, 0)
+
+    wide = jnp.exp(-jnp.abs(param_ref[...]))
+    ratio = wide / (2.0 + wide)
+    ratio_square = ratio * ratio
+    log_sum = jnp.ones_like(ratio) * (1.0 / 17.0)
+    for odd in (15.0, 13.0, 11.0, 9.0, 7.0, 5.0, 3.0, 1.0):
+        log_sum = log_sum * ratio_square + 1.0 / odd
+    rate_ref[...] = -DECAY_MULTIPLIER * (jnp.maximum(-param_ref[...], 0.0) + 2.0 * ratio * log_sum)
 
     size = decay_maps_ref.shape[1]
     per = LANES // size
@@ -568,7 +611,10 @@
             maps[tile, span, index * size : (index + 1) * size] = decay_maps_ref[place]
             maps[tile, span, LANES + index * size : LANES + (index + 1) * size] = input_maps_ref[place]
 
-    relay_all(1, 1)
+    advance(2)
+    for k in range(3, last_raise):
+        y_start(k)
+    advance(3)
     first_y.wait_recv()
     first_pass.start()
 
@@ -579,9 +625,10 @@
             wait_x(k, h)
     first_tp.wait_recv()
 
-    def project(which, token_block, relays):
+    def project(which, token_block, event):
         def body(step, _):
-            relay_at(step, *relays)
+            if event is not None:
+                advance_at(step, event)
             matrix = weights[step // 2, step % 2].reshape(width, block)
             projected[which, step] = jnp.dot(
                 normed[token_block], matrix, preferred_element_type=jnp.float32
@@ -592,9 +639,10 @@
 
     reach = taps_ref.shape[0]
 
-    def recur(which, relays):
+    def recur(which, event):
         def body(step, _):
-            relay_at(step, *relays)
+            if event is not None:
+                advance_at(step, event)
             rows = pl.ds(pl.multiple_of(step * SEQ_LEN, SEQ_LEN), SEQ_LEN)
             for tile in range(tiles):
                 part, lane = tile * LANES // block, tile * LANES % block
@@ -635,12 +683,12 @@
 
         lax.fori_loop(0, tokens // SEQ_LEN, body, 0)
 
-    project(0, y, (2, 0))
-    recur(0, (2, 1))
+    project(0, y, 4)
+    recur(0, None)
     first_pass.wait_recv()
-    project(1, 1 - y, (3, 0))
+    project(1, 1 - y, None)
     offset_copy.wait_recv()
-    recur(1, (4, 0))
+    recur(1, 5)
 
     wait_own(2)
     wait_x(2, 0)
@@ -680,15 +728,11 @@
     mid_copy = y_act(mid_send, mid_got, 6)
     mid_copy.start()
 
-    last_raise = 3 + raises
-    for k in range(5, last_raise):
-        relay_all(k, 0)
-    for k in range(3, last_raise):
-        forward_y(k)
-    for k in range(last_raise, chunks):
-        z_start(k, 0)
+    y_start(last_raise)
+    up = 6
+    for index in range(raises):
+        advance(up + index)
     mix_copy(0).wait_recv()
-    relay_all(3, 1)
 
     mid_copy.wait_recv()
 
@@ -713,20 +757,22 @@
     second_tp, second_y, second_pass = block_copies(normed_mid, 11)
     second_y.start()
     second_tp.start()
-    for k in range(last_raise, chunks):
-        for q in range(2):
-            y_copy(k, q).start()
-
-    for k in range(4, last_raise):
-        relay_all(k, 1)
+    for k in range(last_raise + 1, chunks):
+        y_start(k)
+    for index in range(raises):
+        advance(up + raises + index)
+    down = up + 2 * raises
     for k in range(3, last_raise):
+        if k == last_raise - 1:
+            advance(down)
         wait_own(k)
         wait_x(k, 0)
         wait_x(k, 1)
 
-    def lift(which, token_block, relays):
+    def lift(which, token_block, event):
         def body(step, _):
-            relay_at(step, *relays)
+            if event is not None:
+                advance_at(step, event)
             matrix = weights[3 + step // 2, step % 2].reshape(width, block)
             total = jnp.dot(normed_mid[token_block], matrix, preferred_element_type=jnp.float32)
             lanes = pl.ds(pl.multiple_of(step * block, block), block)
@@ -736,15 +782,13 @@
         lax.fori_loop(0, 2 * raises, body, 0)
 
     second_tp.wait_recv()
-    lift(0, y, (last_raise, 0))
+    lift(0, y, None)
     second_y.wait_recv()
     second_pass.start()
     second_pass.wait_recv()
-    lift(1, 1 - y, (last_raise + 1, 0))
-    for k in range(last_raise + 2, chunks):
-        relay_all(k, 0)
-    for k in range(last_raise, chunks):
-        forward_y(k)
+    lift(1, 1 - y, down + 1)
+    for index in range(2, raises):
+        advance(down + index)
 
     depth = raises * quarter
 
@@ -816,16 +860,37 @@
 
         lax.fori_loop(0, tokens // CHUNK_ROWS, body, 0)
 
-    for k in range(last_raise, chunks):
+    def wait_sends(places):
+        for k in places:
+            for q in range(2):
+                y_copy(k, q).wait_send()
+            for h in range(2):
+                z_copy(k, h, 1).wait_send()
+                z_copy(k, h, 2).wait_send()
+
+                @pl.when(is_mid)
+                def _():
+                    z_copy(k, h, 3).wait_send()
+                    z_relay(k, h).wait_send()
+
+                for m in (1, 2, 3):
+                    x_copy(k, h, m).wait_send()
+
+    order = [(0, m) for m in range(4)] + [(1, m) for m in (0, 2, 3, 1)]
+    far, near = down + raises, down + 2 * raises
+    advance(far)
+    for k in lowers:
         wait_own(k)
         wait_x(k, 0)
-    order = [(0, m) for m in range(4)] + [(1, m) for m in range(4)]
+    wait_sends(range(last_raise))
     for index, (h, m) in enumerate(order):
-        if index == 5:
-            for k in range(last_raise, chunks):
-                relay_all(k, 1)
-            for k in range(last_raise, chunks):
-                wait_x(k, 1)
+        if index in (2, 4):
+            advance(far + index // 2)
+        if index >= 5:
+            advance(near + index - 5)
+        if h == 1 and m:
+            for k in lowers:
+                x_copy(k, 1, m).wait_recv()
         lower(h, m)
         pass_on(h, m)
         if index:
@@ -835,20 +900,7 @@
         for mm in range(2):
             close(h, mm)
 
-    for k in range(chunks):
-        for q in range(2):
-            y_copy(k, q).wait_send()
-        for h in range(2):
-            z_copy(k, h, 1).wait_send()
-            z_copy(k, h, 2).wait_send()
-
-            @pl.when(is_mid)
-            def _():
-                z_copy(k, h, 3).wait_send()
-                z_relay(k, h).wait_send()
-
-            for m in (1, 2, 3):
-                x_copy(k, h, m).wait_send()
+    wait_sends(lowers)
     for copy in (first_tp, first_y, first_pass, second_tp, second_y, second_pass, offset_copy, mid_copy):
         copy.wait_send()
     for phase in range(2):
@@ -889,16 +941,18 @@
     depth = raises * quarter
     tiles = quarter // LANES
     half_type, full_type = jnp.bfloat16, jnp.float32
-    rate = -DECAY_MULTIPLIER * jax.nn.softplus(-channel_decay_param)
     vmem = pl.BlockSpec(memory_space=pltpu.VMEM)
     anywhere = pl.BlockSpec(memory_space=pl.ANY)
     dma = pltpu.SemaphoreType.DMA
     return pl.pallas_call(
         whole_kernel,
         out_shape=jax.ShapeDtypeStruct((tokens, half_width), half_type),
-        in_specs=[vmem] * 8 + [anywhere] * 5,
+        in_specs=[anywhere] * 2 + [vmem] * 6 + [anywhere] * 5,
         out_specs=vmem,
         scratch_shapes=[
+            pltpu.VMEM((tokens, half_width), half_type),
+            pltpu.VMEM((tokens, half_width), full_type),
+            pltpu.VMEM((half_width // LANES, LANES), full_type),
             pltpu.VMEM((chunks, 2, n_fs, block, block), half_type),
             pltpu.VMEM((2, tokens, width), half_type),
             pltpu.VMEM((2, tokens, width), half_type),
@@ -929,6 +983,7 @@
             dma((chunks, 2, 3)),
             dma((22,)),
             dma((22,)),
+            dma((2,)),
         ],
         compiler_params=pltpu.CompilerParams(
             collective_id=0, has_side_effects=True, vmem_limit_bytes=67043328
@@ -942,7 +997,7 @@
         causal_filter_weight,
         decay_gate_matrix,
         input_gate_matrix,
-        rate.reshape(-1, LANES),
+        channel_decay_param.reshape(-1, LANES),
         recurrent_input_weight,
         output_gate_weight,
         recurrent_output_weight,

time: 232 us -> 204 us (0.88)
  Pallas kernels: 226 us -> 201 us
    pallas_call x1, Pallas kernels: 226 us -> 201 us  [whole_layer(): pl.pallas_call(whole_kernel, out_shape=jax.ShapeDtypeStruct((tokens, half...]
where the time goes in v1:
time: 204 us; the launch traced here: 203 us
  Pallas kernels  201 us (99%)
  local copies, waits for them, and re-layouts  2.26 us (1%)
    pallas_call x1, Pallas kernels, whole_layer(): pl.pallas_call(whole_kernel, out_shape=jax.ShapeDtypeStruct((tokens, half...  201 us

profile of v1, /device:TPU:0, one launch (start us, length us, event | category | flops | bytes accessed | tf_op | source)
XLA Modules:
  0.0 203.3 jit_solution(3159561529971396278)
XLA Ops:
  0.0 201.0 %whole_layer.1 = bf16[512,1024]{1,0:T(8,128)(2,1)} custom-call(bf16[512,1024]{1,0:T(8,128)(2,1)} %stream_hbm.1, f32[512,1024]{1,0:T(8,128)} %offset_hbm.1, f32[16,128]{1,0:T(8,128)} %bitcast.3, f32[16,128]{1,0:T(8,128)} %bitcast.4, bf16[4,1024]{1,0:T(4,128)(2,1)} %taps_ref.1, bf16[16,64,64]{2,1,0:T(8,128)(2,1)} %decay_maps_ref.1, ...), custom_call_target="tpu_custom_call" | custom-call | tf_op jit(solution)/shard_map/whole_layer/pallas_call | solution.py:947
  201.0 2.3 %copy.15 = bf16[512,1024]{1,0:T(8,128)(2,1)} copy(bf16[512,1024]{1,0:T(8,128)(2,1)} %whole_layer.1) | data formatting | bytes 2097152

commit v2 on v1

--- a/solution.py
+++ b/solution.py
@@ -317,7 +317,12 @@
 
 MESH = pl.DeviceIdType.MESH
 CHUNK_ROWS = 128
-AHEAD = (2, 2, 2, 3)
+AHEAD = (1, 1, 1, 2, 3)
+END_AHEAD = (1, 1, 1, 2, 3)
+LEAD = 2
+END_ORDER = (
+    (0, 1), (0, 2), (1, 1), (0, 3), (1, 2), (2, 1), (1, 3), (2, 2), (3, 1), (2, 3), (3, 2), (3, 3),
+)
 
 
 def whole_kernel(
@@ -378,7 +383,10 @@
     quarter = half_width // 2
     lane_tiles = half_width // LANES
     raises = (chunks - 3) // 2
+    last_raise = 3 + raises
+    lowers = range(last_raise, chunks)
     is_mid = jnp.logical_or(z == 1, z == 2)
+    is_end = jnp.logical_not(is_mid)
     low = (z // 2) == tp
 
     def plane(m):
@@ -427,42 +435,58 @@
     def local_copy(k, q):
         part = part_of(q)
         return pltpu.make_async_copy(
-            shard_block(k, y, part), weights.at[k, part, fs], local_sem.at[k, q]
+            shard_block(k, y, part), weights.at[k, part, fs], local_sem.at[0]
         )
+
+    def group_of(k):
+        return 0 if k < 2 else 1 if k == 2 else 2 if k < last_raise else 3
+
+    def y_slot(k, q):
+        return k if q == 0 else chunks + group_of(k)
+
+    def x_slot(k, h, m):
+        if k < last_raise:
+            return group_of(k) if k < 3 else k - 1
+        return 1 + raises + (1 if h == 0 else 1 + m)
+
+    def count_wait(ref, sem):
+        pltpu.make_async_copy(ref, ref, sem).wait()
 
     def y_copy(k, q):
         part = part_of(q)
         return remote(
-            shard_block(k, 1 - y, part), weights.at[k, part, fs], y_send.at[k, q], y_recv.at[k, q], y_peer
+            shard_block(k, 1 - y, part), weights.at[k, part, fs], y_send.at[0], y_recv.at[y_slot(k, q)], y_peer
         )
 
     def z_copy(k, h, m):
         spot = weights.at[k, rep, fs if h == 0 else 2 * z + 1 - y]
         src = shard_block(k, y, rep) if h == 0 else spot
-        return remote(src, spot, z_send.at[k, h, m - 1], z_recv.at[k, h, m - 1], z_peer(m))
+        return remote(src, spot, z_send.at[0], z_recv.at[k, h, m - 1], z_peer(m))
 
     def z_relay(k, h):
         spot = weights.at[k, rep, 2 * plane(2) + (y if h == 0 else 1 - y)]
-        return remote(spot, spot, z_send.at[k, h, 3], z_recv.at[k, h, 2], z_peer(1))
+        return remote(spot, spot, z_send.at[0], z_recv.at[k, h, 2], z_peer(1))
 
     def x_copy(k, h, m):
         spot = weights.at[k, rep, 2 * plane(m) + (y if h == 0 else 1 - y)]
-        return remote(spot, spot, x_send.at[k, h, m - 1], x_recv.at[k, h, m - 1], x_peer)
-
-    last_raise = 3 + raises
-    lowers = range(last_raise, chunks)
+        return remote(spot, spot, x_send.at[0], x_recv.at[x_slot(k, h, m)], x_peer)
+
     every = (2, 1, 3)
     events = [(k, h, every) for k, h in ((0, 0), (1, 0), (0, 1), (1, 1), (2, 0), (2, 1))]
     events += [(k, h, every) for h in range(2) for k in range(3, last_raise)]
     events += [(k, 0, every) for k in lowers]
     events += [(k, 1, (2, 3)) for k in lowers] + [(k, 1, (1,)) for k in lowers]
 
-    def reach_of(index):
-        return index + AHEAD[min(index, len(AHEAD) - 1)]
-
     def start_after(index):
-        for later in range(reach_of(index - 1) + 1 if index else 2, reach_of(index) + 1):
-            start(later)
+        for role, ahead in ((is_mid, AHEAD), (is_end, END_AHEAD)):
+
+            def reach_of(place, ahead=ahead):
+                return place + ahead[min(place, len(ahead) - 1)] if place >= 0 else 0
+
+            @pl.when(role)
+            def _():
+                for later in range(reach_of(index - 1) + 1, reach_of(index) + 1):
+                    start(later)
 
     def start(index):
         if index >= len(events):
@@ -471,7 +495,13 @@
         if h == 1 and 2 in sources:
             y_copy(k, 0).wait_recv()
         for m in sources:
-            if m < 3:
+            if m == 1 and sources == every and index >= 1:
+
+                @pl.when(is_end)
+                def _():
+                    z_copy(k, h, 1).start()
+
+            elif m < 3:
                 z_copy(k, h, m).start()
             else:
 
@@ -479,40 +509,47 @@
                 def _():
                     z_copy(k, h, 3).start()
 
-    def relay(k, h, m):
+    def relay(index, m):
+        k, h, _ = events[index]
         z_copy(k, h, m).wait_recv()
         x_copy(k, h, m).start()
 
         @pl.when(jnp.logical_and(is_mid, m == 2))
         def _():
             z_relay(k, h).start()
+            lead = index + (1 if index < 2 else LEAD)
+            for place in (lead,) if index != 2 else (lead - 1, lead):
+                next_k, next_h, next_sources = events[min(place, len(events) - 1)]
+                if next_sources == every:
+                    z_copy(next_k, next_h, 1).start()
 
     def advance(index):
-        k, h, sources = events[index]
-        for place, m in enumerate(sorted(sources)):
-            relay(k, h, m)
+        for place, m in enumerate(sorted(events[index][2])):
+            relay(index, m)
             if place == 0:
                 start_after(index)
 
-    def advance_at(step, index):
-        k, h, _ = events[index]
-
-        @pl.when(step < 3)
+    def advance_for(role, index):
+        @pl.when(role)
         def _():
-            relay(k, h, step + 1)
-
-        @pl.when(step == 0)
+            advance(index)
+
+    def advance_at(step, role, index):
+        @pl.when(jnp.logical_and(role, step < 3))
+        def _():
+            relay(index, step + 1)
+
+        @pl.when(jnp.logical_and(role, step == 0))
         def _():
             start_after(index)
 
-    def wait_own(k):
-        for q in range(2):
-            local_copy(k, q).wait()
-        y_copy(k, 1).wait_recv()
-
-    def wait_x(k, h):
-        for m in (1, 2, 3):
-            x_copy(k, h, m).wait_recv()
+    def wait_y(first, last):
+        count_wait(weights.at[first:last, 0, 0], y_recv.at[y_slot(first, 1)])
+
+    def wait_x(first, last, h, sources):
+        parts = 1 if h is not None else 2
+        sample = weights.at[first:last, 0:parts, 0 : len(sources)]
+        count_wait(sample, x_recv.at[x_slot(first, h, sources[0])])
 
     def tp_copy(src, dst, slot):
         return remote(src, dst, act_send.at[slot], act_recv.at[slot], t_peer)
@@ -520,13 +557,15 @@
     def y_act(src, dst, slot):
         return remote(src, dst, act_send.at[slot], act_recv.at[slot], y_peer)
 
-    def y_start(k):
-        for q in range(2):
-            y_copy(k, q).start()
-
-    y_start(0)
-    y_start(1)
+    def y_start(places, parts=(0, 1)):
+        for q in parts:
+            for k in places:
+                y_copy(k, q).start()
+
+    y_start((0,), (0,))
     start(0)
+    y_start((1,), (0,))
+    y_start((0, 1), (1,))
     for k in range(chunks):
         for q in range(2):
             local_copy(k, q).start()
@@ -585,13 +624,7 @@
     first_tp.start()
     offset_copy = y_act(offset_send, offsets.at[1], 3)
 
-    y_start(2)
-    start(1)
-    advance(0)
-    first_y.start()
-    advance(1)
-    offset_copy.start()
-
+    y_start((2,))
     wide = jnp.exp(-jnp.abs(param_ref[...]))
     ratio = wide / (2.0 + wide)
     ratio_square = ratio * ratio
@@ -611,24 +644,42 @@
             maps[tile, span, index * size : (index + 1) * size] = decay_maps_ref[place]
             maps[tile, span, LANES + index * size : LANES + (index + 1) * size] = input_maps_ref[place]
 
-    advance(2)
-    for k in range(3, last_raise):
-        y_start(k)
-    advance(3)
+    @pl.when(is_mid)
+    def _():
+        advance(0)
+        first_y.start()
+        advance(1)
+        offset_copy.start()
+        advance(2)
+        y_start(range(3, last_raise))
+        advance(3)
+
+    @pl.when(is_end)
+    def _():
+        for place, (index, m) in enumerate(END_ORDER):
+            relay(index, m)
+            if m == 1:
+                start_after(index)
+            if place == 1:
+                first_y.start()
+            if place == 4:
+                offset_copy.start()
+            if place == 7:
+                y_start(range(3, last_raise))
+
     first_y.wait_recv()
     first_pass.start()
 
-    for k in range(2):
-        wait_own(k)
-    for k in range(2):
-        for h in range(2):
-            wait_x(k, h)
+    count_wait(weights.at[:, :, 0], local_sem.at[0])
+    wait_y(0, 2)
+    advance_for(is_mid, 4)
+    wait_x(0, 2, None, every)
     first_tp.wait_recv()
 
-    def project(which, token_block, event):
+    def project(which, token_block, *relays):
         def body(step, _):
-            if event is not None:
-                advance_at(step, event)
+            for role, index in relays:
+                advance_at(step, role, index)
             matrix = weights[step // 2, step % 2].reshape(width, block)
             projected[which, step] = jnp.dot(
                 normed[token_block], matrix, preferred_element_type=jnp.float32
@@ -639,10 +690,10 @@
 
     reach = taps_ref.shape[0]
 
-    def recur(which, event):
+    def recur(which, *relays):
         def body(step, _):
-            if event is not None:
-                advance_at(step, event)
+            for role, index in relays:
+                advance_at(step, role, index)
             rows = pl.ds(pl.multiple_of(step * SEQ_LEN, SEQ_LEN), SEQ_LEN)
             for tile in range(tiles):
                 part, lane = tile * LANES // block, tile * LANES % block
@@ -683,19 +734,22 @@
 
         lax.fori_loop(0, tokens // SEQ_LEN, body, 0)
 
-    project(0, y, 4)
-    recur(0, None)
+    project(0, y, (is_end, 4))
+    recur(0)
     first_pass.wait_recv()
-    project(1, 1 - y, None)
+    project(1, 1 - y, (is_mid, 5))
     offset_copy.wait_recv()
-    recur(1, 5)
-
-    wait_own(2)
-    wait_x(2, 0)
-    wait_x(2, 1)
-
-    def mix_out(which):
+    recur(1, (is_end, 5))
+
+    advance_for(is_mid, 6)
+    wait_y(2, 3)
+    wait_x(2, 3, None, every)
+
+    def mix_out(which, *relays):
         def body(step, _):
+            for role, index in relays:
+                advance_at(step, role, index)
+
             def term(place):
                 matrix = weights[2, :, place].reshape(quarter, block)
                 return jnp.dot(mixed[which], matrix, preferred_element_type=jnp.float32).astype(jnp.bfloat16)
@@ -711,7 +765,7 @@
     def mix_copy(which):
         return tp_copy(passed.at[which], got.at[which], 4 + which)
 
-    mix_out(1)
+    mix_out(1, (is_end, 6))
     mix_copy(1).start()
     mix_out(0)
     mix_copy(0).start()
@@ -727,12 +781,14 @@
     lax.fori_loop(0, tokens // CHUNK_ROWS, add_peer, 0)
     mid_copy = y_act(mid_send, mid_got, 6)
     mid_copy.start()
-
-    y_start(last_raise)
+    y_start(lowers, (0,))
+
     up = 6
-    for index in range(raises):
+    for index in range(1, raises):
         advance(up + index)
     mix_copy(0).wait_recv()
+    advance(up + raises)
+    advance_for(is_mid, up + raises + 1)
 
     mid_copy.wait_recv()
 
@@ -757,22 +813,20 @@
     second_tp, second_y, second_pass = block_copies(normed_mid, 11)
     second_y.start()
     second_tp.start()
-    for k in range(last_raise + 1, chunks):
-        y_start(k)
-    for index in range(raises):
+    advance_for(is_end, up + raises + 1)
+    for index in range(2, raises):
         advance(up + raises + index)
     down = up + 2 * raises
+    wait_y(3, last_raise)
     for k in range(3, last_raise):
         if k == last_raise - 1:
             advance(down)
-        wait_own(k)
-        wait_x(k, 0)
-        wait_x(k, 1)
-
-    def lift(which, token_block, event):
+        wait_x(k, k + 1, None, every)
+
+    def lift(which, token_block, *relays):
         def body(step, _):
-            if event is not None:
-                advance_at(step, event)
+            for role, index in relays:
+                advance_at(step, role, index)
             matrix = weights[3 + step // 2, step % 2].reshape(width, block)
             total = jnp.dot(normed_mid[token_block], matrix, preferred_element_type=jnp.float32)
             lanes = pl.ds(pl.multiple_of(step * block, block), block)
@@ -782,12 +836,15 @@
         lax.fori_loop(0, 2 * raises, body, 0)
 
     second_tp.wait_recv()
-    lift(0, y, None)
+    lift(0, y)
+    advance_for(is_mid, down + 1)
     second_y.wait_recv()
+    y_start(lowers, (1,))
     second_pass.start()
     second_pass.wait_recv()
-    lift(1, 1 - y, down + 1)
-    for index in range(2, raises):
+    lift(1, 1 - y, (is_end, down + 1), (is_mid, down + 2))
+    advance_for(is_end, down + 2)
+    for index in range(3, raises):
         advance(down + index)
 
     depth = raises * quarter
@@ -860,47 +917,36 @@
 
         lax.fori_loop(0, tokens // CHUNK_ROWS, body, 0)
 
-    def wait_sends(places):
-        for k in places:
-            for q in range(2):
-                y_copy(k, q).wait_send()
-            for h in range(2):
-                z_copy(k, h, 1).wait_send()
-                z_copy(k, h, 2).wait_send()
-
-                @pl.when(is_mid)
-                def _():
-                    z_copy(k, h, 3).wait_send()
-                    z_relay(k, h).wait_send()
-
-                for m in (1, 2, 3):
-                    x_copy(k, h, m).wait_send()
-
     order = [(0, m) for m in range(4)] + [(1, m) for m in (0, 2, 3, 1)]
     far, near = down + raises, down + 2 * raises
     advance(far)
-    for k in lowers:
-        wait_own(k)
-        wait_x(k, 0)
-    wait_sends(range(last_raise))
+    wait_y(last_raise, chunks)
+    wait_x(last_raise, chunks, 0, every)
     for index, (h, m) in enumerate(order):
         if index in (2, 4):
             advance(far + index // 2)
         if index >= 5:
             advance(near + index - 5)
         if h == 1 and m:
-            for k in lowers:
-                x_copy(k, 1, m).wait_recv()
+            wait_x(last_raise, chunks, 1, (m,))
         lower(h, m)
         pass_on(h, m)
-        if index:
+        if index and index < 5:
             finish(*order[index - 1])
-    finish(*order[-1])
+        if index >= 4:
+            finish(h, m)
     for h in range(2):
         for mm in range(2):
             close(h, mm)
 
-    wait_sends(lowers)
+    count_wait(weights.at[:, :, 0], y_send.at[0])
+    count_wait(weights.at[:, 0, 0:6], x_send.at[0])
+    count_wait(weights.at[:, 0, 0:4], z_send.at[0])
+
+    @pl.when(is_mid)
+    def _():
+        count_wait(weights.at[:, 0, 0:4], z_send.at[0])
+
     for copy in (first_tp, first_y, first_pass, second_tp, second_y, second_pass, offset_copy, mid_copy):
         copy.wait_send()
     for phase in range(2):
@@ -974,13 +1020,13 @@
             pltpu.VMEM((2, 2, 2, tokens, block), half_type),
             pltpu.VMEM((2, 2, tokens, block), half_type),
             pltpu.VMEM((2, 2, tokens, block), half_type),
-            dma((chunks, 2)),
-            dma((chunks, 2)),
-            dma((chunks, 2)),
-            dma((chunks, 2, 4)),
+            dma((1,)),
+            dma((1,)),
+            dma((chunks + 4,)),
+            dma((1,)),
             dma((chunks, 2, 3)),
-            dma((chunks, 2, 3)),
-            dma((chunks, 2, 3)),
+            dma((1,)),
+            dma((raises + 6,)),
             dma((22,)),
             dma((22,)),
             dma((2,)),
@@ -1013,7 +1059,7 @@
         and half_width % (8 * LANES) == 0
         and tokens % (4 * SEQ_LEN) == 0
         and up_projection_weight.shape[1] % half_width == 0
-        and up_projection_weight.shape[1] // half_width >= 2
+        and up_projection_weight.shape[1] // half_width >= 3
         and LANES % decay_gate_matrix.shape[1] == 0
     )
 

time: 204 us -> 194 us (0.951)
  Pallas kernels: 201 us -> 192 us
    pallas_call x1, Pallas kernels: 201 us -> 192 us  [whole_layer(): pl.pallas_call(whole_kernel, out_shape=jax.ShapeDtypeStruct((tokens, half...]
where the time goes in v2:
time: 194 us
  Pallas kernels  192 us (99%)
  local copies, waits for them, and re-layouts  2.26 us (1%)
    pallas_call x1, Pallas kernels, whole_layer(): pl.pallas_call(whole_kernel, out_shape=jax.ShapeDtypeStruct((tokens, half...  192 us

profile of v2, /device:TPU:0, one launch (start us, length us, event | category | flops | bytes accessed | tf_op | source)
XLA Modules:
  0.0 194.3 jit_solution(15244327267334987704)
XLA Ops:
  0.0 192.0 %whole_layer.1 = bf16[512,1024]{1,0:T(8,128)(2,1)} custom-call(bf16[512,1024]{1,0:T(8,128)(2,1)} %stream_hbm.1, f32[512,1024]{1,0:T(8,128)} %offset_hbm.1, f32[16,128]{1,0:T(8,128)} %bitcast.3, f32[16,128]{1,0:T(8,128)} %bitcast.4, bf16[4,1024]{1,0:T(4,128)(2,1)} %taps_ref.1, bf16[16,64,64]{2,1,0:T(8,128)(2,1)} %decay_maps_ref.1, ...), custom_call_target="tpu_custom_call" | custom-call | tf_op jit(solution)/shard_map/whole_layer/pallas_call | solution.py:993
  192.0 2.3 %copy.15 = bf16[512,1024]{1,0:T(8,128)(2,1)} copy(bf16[512,1024]{1,0:T(8,128)(2,1)} %whole_layer.1) | data formatting | bytes 2097152

commit v3 on v2

--- a/solution.py
+++ b/solution.py
@@ -317,11 +317,12 @@
 
 MESH = pl.DeviceIdType.MESH
 CHUNK_ROWS = 128
-AHEAD = (1, 1, 1, 2, 3)
-END_AHEAD = (1, 1, 1, 2, 3)
+AHEAD = (1, 1, 1, 1, 2, 3)
+END_AHEAD = (1, 1, 1, 1, 2, 3)
+STEADY = 4
 LEAD = 2
 END_ORDER = (
-    (0, 1), (0, 2), (1, 1), (0, 3), (1, 2), (2, 1), (1, 3), (2, 2), (3, 1), (2, 3), (3, 2), (3, 3),
+    (0, 1), (0, 2), (0, 3), (1, 2), (1, 1), (1, 3), (2, 2), (2, 1), (2, 3), (3, 2), (3, 1), (3, 3),
 )
 
 
@@ -362,6 +363,7 @@
     activity,
     partial,
     partial_got,
+    total,
     last_send,
     last_got,
     local_sem,
@@ -447,7 +449,7 @@
     def x_slot(k, h, m):
         if k < last_raise:
             return group_of(k) if k < 3 else k - 1
-        return 1 + raises + (1 if h == 0 else 1 + m)
+        return 2 + raises + (0 if h == 0 else m - 1 if m > 1 else 3 + k - last_raise)
 
     def count_wait(ref, sem):
         pltpu.make_async_copy(ref, ref, sem).wait()
@@ -472,6 +474,7 @@
         return remote(spot, spot, x_send.at[0], x_recv.at[x_slot(k, h, m)], x_peer)
 
     every = (2, 1, 3)
+    up = 6
     events = [(k, h, every) for k, h in ((0, 0), (1, 0), (0, 1), (1, 1), (2, 0), (2, 1))]
     events += [(k, h, every) for h in range(2) for k in range(3, last_raise)]
     events += [(k, 0, every) for k in lowers]
@@ -495,7 +498,7 @@
         if h == 1 and 2 in sources:
             y_copy(k, 0).wait_recv()
         for m in sources:
-            if m == 1 and sources == every and index >= 1:
+            if m == 1 and index >= 1:
 
                 @pl.when(is_end)
                 def _():
@@ -517,17 +520,39 @@
         @pl.when(jnp.logical_and(is_mid, m == 2))
         def _():
             z_relay(k, h).start()
-            lead = index + (1 if index < 2 else LEAD)
-            for place in (lead,) if index != 2 else (lead - 1, lead):
+            lead = index + (1 if index < STEADY else LEAD)
+            for place in (lead,) if index != STEADY else (lead - 1, lead):
                 next_k, next_h, next_sources = events[min(place, len(events) - 1)]
                 if next_sources == every:
                     z_copy(next_k, next_h, 1).start()
+            far_step = index - up - 3 * raises
+            if far_step == raises - 2:
+                z_copy(last_raise, 1, 1).start()
+            if far_step == raises - 1:
+                for later_k in range(last_raise + 1, chunks):
+                    z_copy(later_k, 1, 1).start()
 
     def advance(index):
         for place, m in enumerate(sorted(events[index][2])):
             relay(index, m)
             if place == 0:
                 start_after(index)
+
+    def skewed(index):
+        relay(index, 1)
+        start_after(index)
+        relay(index, 2)
+        if index > up:
+            relay(index - 1, 3)
+
+    def advance_both(index):
+        @pl.when(is_mid)
+        def _():
+            skewed(index)
+
+        @pl.when(is_end)
+        def _():
+            advance(index)
 
     def advance_for(role, index):
         @pl.when(role)
@@ -658,7 +683,7 @@
     def _():
         for place, (index, m) in enumerate(END_ORDER):
             relay(index, m)
-            if m == 1:
+            if place % 3 == 0:
                 start_after(index)
             if place == 1:
                 first_y.start()
@@ -741,7 +766,11 @@
     offset_copy.wait_recv()
     recur(1, (is_end, 5))
 
-    advance_for(is_mid, 6)
+
+    @pl.when(is_mid)
+    def _():
+        skewed(up)
+
     wait_y(2, 3)
     wait_x(2, 3, None, every)
 
@@ -783,12 +812,16 @@
     mid_copy.start()
     y_start(lowers, (0,))
 
-    up = 6
-    for index in range(1, raises):
-        advance(up + index)
+    for index in range(1, raises + 1):
+        advance_both(up + index)
     mix_copy(0).wait_recv()
-    advance(up + raises)
-    advance_for(is_mid, up + raises + 1)
+    relay(up + raises + 1, 1)
+    start_after(up + raises + 1)
+    relay(up + raises + 1, 2)
+
+    @pl.when(is_mid)
+    def _():
+        relay(up + raises, 3)
 
     mid_copy.wait_recv()
 
@@ -813,14 +846,23 @@
     second_tp, second_y, second_pass = block_copies(normed_mid, 11)
     second_y.start()
     second_tp.start()
-    advance_for(is_end, up + raises + 1)
+
+    @pl.when(is_end)
+    def _():
+        relay(up + raises + 1, 3)
+
     for index in range(2, raises):
-        advance(up + raises + index)
+        advance_both(up + raises + index)
     down = up + 2 * raises
     wait_y(3, last_raise)
     for k in range(3, last_raise):
         if k == last_raise - 1:
-            advance(down)
+            advance_both(down)
+
+            @pl.when(is_mid)
+            def _():
+                skewed(down + 1)
+
         wait_x(k, k + 1, None, every)
 
     def lift(which, token_block, *relays):
@@ -837,13 +879,19 @@
 
     second_tp.wait_recv()
     lift(0, y)
-    advance_for(is_mid, down + 1)
+
+    @pl.when(is_mid)
+    def _():
+        skewed(down + 2)
+
+    advance_for(is_end, down + 1)
+
     second_y.wait_recv()
     y_start(lowers, (1,))
     second_pass.start()
     second_pass.wait_recv()
-    lift(1, 1 - y, (is_end, down + 1), (is_mid, down + 2))
-    advance_for(is_end, down + 2)
+    lift(1, 1 - y, (is_end, down + 2))
+
     for index in range(3, raises):
         advance(down + index)
 
@@ -886,7 +934,7 @@
     def finish(h, m):
         @pl.when(is_owner(m))
         def _():
-            owner_copy(h, m).wait_recv()
+            (last_part(1) if (h, m) == (1, 1) else owner_copy(h, m)).wait_recv()
 
             def body(step, _):
                 rows = pl.ds(pl.multiple_of(step * CHUNK_ROWS, CHUNK_ROWS), CHUNK_ROWS)
@@ -898,6 +946,31 @@
 
             lax.fori_loop(0, tokens // CHUNK_ROWS, body, 0)
             last_copy(h, m).start()
+
+    def last_part(which):
+        return tp_copy(partial.at[1, 1, which], partial_got.at[1, 1, which], 17 if which else 22)
+
+    def lower_last():
+        place = 2 * plane(1) + 1 - y
+        split = (raises - 1) * quarter
+        for k in range(last_raise, chunks - 1):
+            wait_x(k, k + 1, 1, (1,))
+
+        def early(which, _):
+            matrix = weights[last_raise : chunks - 1, :, place].reshape(split, block)
+            total[which] = jnp.dot(activity[which, :, :split], matrix, preferred_element_type=jnp.float32)
+            return 0
+
+        lax.fori_loop(0, 2, early, 0)
+        wait_x(chunks - 1, chunks, 1, (1,))
+        for which in (1, 0):
+            matrix = weights[chunks - 1, :, place].reshape(quarter, block)
+            term = jnp.dot(activity[which, :, split:], matrix, preferred_element_type=jnp.float32)
+            partial[1, 1, which] = (total[which] + term).astype(jnp.bfloat16)
+
+            @pl.when(jnp.logical_not(low))
+            def _():
+                last_part(which).start()
 
     def close(h, mm):
         owned = mm + 2 * (1 - low.astype(jnp.int32))
@@ -919,14 +992,43 @@
 
     order = [(0, m) for m in range(4)] + [(1, m) for m in (0, 2, 3, 1)]
     far, near = down + raises, down + 2 * raises
-    advance(far)
+
+    def first_far(index):
+        relay(index, 2)
+        start_after(index)
+
+    @pl.when(is_mid)
+    def _():
+        first_far(far)
+        relay(far - 1, 3)
+        first_far(far + 1)
+        relay(far, 3)
+
+    advance_for(is_end, far)
     wait_y(last_raise, chunks)
     wait_x(last_raise, chunks, 0, every)
     for index, (h, m) in enumerate(order):
+        if index == 2:
+
+            @pl.when(is_mid)
+            def _():
+                first_far(far + 2)
+                relay(far + 1, 3)
+
+        if index == 4:
+
+            @pl.when(is_mid)
+            def _():
+                relay(far + 2, 3)
+
         if index in (2, 4):
-            advance(far + index // 2)
+            advance_for(is_end, far + index // 2)
         if index >= 5:
             advance(near + index - 5)
+        if (h, m) == (1, 1):
+            lower_last()
+            finish(1, 1)
+            continue
         if h == 1 and m:
             wait_x(last_raise, chunks, 1, (m,))
         lower(h, m)
@@ -935,9 +1037,15 @@
             finish(*order[index - 1])
         if index >= 4:
             finish(h, m)
-    for h in range(2):
-        for mm in range(2):
-            close(h, mm)
+    close(1, 0)
+    close(0, 0)
+
+    @pl.when(low)
+    def _():
+        last_part(0).wait_recv()
+
+    close(1, 1)
+    close(0, 1)
 
     count_wait(weights.at[:, :, 0], y_send.at[0])
     count_wait(weights.at[:, 0, 0:6], x_send.at[0])
@@ -960,7 +1068,11 @@
 
         @pl.when(jnp.logical_not(is_owner(m)))
         def _():
-            owner_copy(h, m).wait_send()
+            if (h, m) == (1, 1):
+                last_part(0).wait_send()
+                last_part(1).wait_send()
+            else:
+                owner_copy(h, m).wait_send()
 
 
 def whole_layer(
@@ -1018,6 +1130,7 @@
             pltpu.VMEM((2, tokens, depth), half_type),
             pltpu.VMEM((4, 2, 2, tokens, block), half_type),
             pltpu.VMEM((2, 2, 2, tokens, block), half_type),
+            pltpu.VMEM((2, tokens, block), full_type),
             pltpu.VMEM((2, 2, tokens, block), half_type),
             pltpu.VMEM((2, 2, tokens, block), half_type),
             dma((1,)),
@@ -1026,9 +1139,9 @@
             dma((1,)),
             dma((chunks, 2, 3)),
             dma((1,)),
-            dma((raises + 6,)),
-            dma((22,)),
-            dma((22,)),
+            dma((2 * raises + 5,)),
+            dma((23,)),
+            dma((23,)),
             dma((2,)),
         ],
         compiler_params=pltpu.CompilerParams(

time: 194 us -> 188 us (0.969)
  Pallas kernels: 192 us -> 186 us
    pallas_call x1, Pallas kernels: 192 us -> 186 us  [whole_layer(): pl.pallas_call(whole_kernel, out_shape=jax.ShapeDtypeStruct((tokens, half...]
where the time goes in v3:
time: 188 us
  Pallas kernels  186 us (99%)
  local copies, waits for them, and re-layouts  2.26 us (1%)
    pallas_call x1, Pallas kernels, whole_layer(): pl.pallas_call(whole_kernel, out_shape=jax.ShapeDtypeStruct((tokens, half...  186 us

profile of v3, /device:TPU:0, one launch (start us, length us, event | category | flops | bytes accessed | tf_op | source)
XLA Modules:
  0.0 188.0 jit_solution(18063678577258591713)
XLA Ops:
  0.0 185.7 %whole_layer.1 = bf16[512,1024]{1,0:T(8,128)(2,1)} custom-call(bf16[512,1024]{1,0:T(8,128)(2,1)} %stream_hbm.1, f32[512,1024]{1,0:T(8,128)} %offset_hbm.1, f32[16,128]{1,0:T(8,128)} %bitcast.3, f32[16,128]{1,0:T(8,128)} %bitcast.4, bf16[4,1024]{1,0:T(4,128)(2,1)} %taps_ref.1, bf16[16,64,64]{2,1,0:T(8,128)(2,1)} %decay_maps_ref.1, ...), custom_call_target="tpu_custom_call" | custom-call | tf_op jit(solution)/shard_map/whole_layer/pallas_call | solution.py:1105
  185.7 2.3 %copy.15 = bf16[512,1024]{1,0:T(8,128)(2,1)} copy(bf16[512,1024]{1,0:T(8,128)(2,1)} %whole_layer.1) | data formatting | bytes 2097152

commit v4 on v3

--- a/solution.py
+++ b/solution.py
@@ -318,7 +318,6 @@
 MESH = pl.DeviceIdType.MESH
 CHUNK_ROWS = 128
 AHEAD = (1, 1, 1, 1, 2, 3)
-END_AHEAD = (1, 1, 1, 1, 2, 3)
 STEADY = 4
 LEAD = 2
 END_ORDER = (
@@ -329,12 +328,12 @@
 def whole_kernel(
     stream_hbm,
     offset_hbm,
-    first_gain_ref,
-    second_gain_ref,
-    taps_ref,
-    decay_maps_ref,
-    input_maps_ref,
-    param_ref,
+    first_gain_hbm,
+    second_gain_hbm,
+    taps_hbm,
+    decay_maps_hbm,
+    input_maps_hbm,
+    param_hbm,
     value_hbm,
     gate_hbm,
     output_hbm,
@@ -343,6 +342,12 @@
     out_ref,
     stream_ref,
     offset_ref,
+    first_gain_ref,
+    second_gain_ref,
+    taps_ref,
+    decay_maps_ref,
+    input_maps_ref,
+    param_ref,
     rate_ref,
     weights,
     normed,
@@ -401,10 +406,20 @@
     def z_peer(m):
         return (rep, 2 * plane(m) + y, tp)
 
-    loads = (
-        pltpu.make_async_copy(stream_hbm, stream_ref, load_sem.at[0]),
-        pltpu.make_async_copy(offset_hbm, offset_ref, load_sem.at[1]),
+    places = (
+        (stream_hbm, stream_ref),
+        (first_gain_hbm, first_gain_ref),
+        (offset_hbm, offset_ref),
+        (second_gain_hbm, second_gain_ref),
+        (taps_hbm, taps_ref),
+        (decay_maps_hbm, decay_maps_ref),
+        (input_maps_hbm, input_maps_ref),
+        (param_hbm, param_ref),
     )
+    loads = [
+        pltpu.make_async_copy(source, target, load_sem.at[index])
+        for index, (source, target) in enumerate(places)
+    ]
     for load in loads:
         load.start()
 
@@ -481,15 +496,18 @@
     events += [(k, 1, (2, 3)) for k in lowers] + [(k, 1, (1,)) for k in lowers]
 
     def start_after(index):
-        for role, ahead in ((is_mid, AHEAD), (is_end, END_AHEAD)):
-
-            def reach_of(place, ahead=ahead):
-                return place + ahead[min(place, len(ahead) - 1)] if place >= 0 else 0
-
-            @pl.when(role)
-            def _():
-                for later in range(reach_of(index - 1) + 1, reach_of(index) + 1):
-                    start(later)
+        def reach_of(place):
+            return place + AHEAD[min(place, len(AHEAD) - 1)] if place >= 0 else 0
+
+        for later in range(reach_of(index - 1) + 1, reach_of(index) + 1):
+            if later == STEADY + 1:
+
+                @pl.when(is_mid)
+                def _():
+                    start(STEADY + 1)
+
+            else:
+                start(later)
 
     def start(index):
         if index >= len(events):
@@ -559,14 +577,16 @@
         def _():
             advance(index)
 
-    def advance_at(step, role, index):
-        @pl.when(jnp.logical_and(role, step < 3))
+    def advance_at(step, role, index, first=1, last=3):
+        @pl.when(jnp.logical_and(role, jnp.logical_and(step + 1 >= first, step + 1 <= last)))
         def _():
             relay(index, step + 1)
 
-        @pl.when(jnp.logical_and(role, step == 0))
-        def _():
-            start_after(index)
+        if first == 1:
+
+            @pl.when(jnp.logical_and(role, step == 0))
+            def _():
+                start_after(index)
 
     def wait_y(first, last):
         count_wait(weights.at[first:last, 0, 0], y_recv.at[y_slot(first, 1)])
@@ -636,9 +656,11 @@
         )
 
     loads[0].wait()
+    loads[1].wait()
     squares(stream_ref, 0)
     square_copy(0).start()
-    loads[1].wait()
+    for load in loads[2:]:
+        load.wait()
     mine = pl.ds(pl.multiple_of(y * quarter, quarter), quarter)
     peers = pl.ds(pl.multiple_of((1 - y) * quarter, quarter), quarter)
     offset_send[...] = offset_ref[:, peers].astype(jnp.bfloat16)
@@ -691,6 +713,7 @@
                 offset_copy.start()
             if place == 7:
                 y_start(range(3, last_raise))
+        start(STEADY + 1)
 
     first_y.wait_recv()
     first_pass.start()
@@ -703,8 +726,8 @@
 
     def project(which, token_block, *relays):
         def body(step, _):
-            for role, index in relays:
-                advance_at(step, role, index)
+            for role, *steps in relays:
+                advance_at(step, role, *steps)
             matrix = weights[step // 2, step % 2].reshape(width, block)
             projected[which, step] = jnp.dot(
                 normed[token_block], matrix, preferred_element_type=jnp.float32
@@ -717,8 +740,8 @@
 
     def recur(which, *relays):
         def body(step, _):
-            for role, index in relays:
-                advance_at(step, role, index)
+            for role, *steps in relays:
+                advance_at(step, role, *steps)
             rows = pl.ds(pl.multiple_of(step * SEQ_LEN, SEQ_LEN), SEQ_LEN)
             for tile in range(tiles):
                 part, lane = tile * LANES // block, tile * LANES % block
@@ -760,9 +783,9 @@
         lax.fori_loop(0, tokens // SEQ_LEN, body, 0)
 
     project(0, y, (is_end, 4))
-    recur(0)
+    recur(0, (is_mid, 5, 1, 2))
     first_pass.wait_recv()
-    project(1, 1 - y, (is_mid, 5))
+    project(1, 1 - y, (is_mid, 5, 3, 3))
     offset_copy.wait_recv()
     recur(1, (is_end, 5))
 
@@ -776,8 +799,8 @@
 
     def mix_out(which, *relays):
         def body(step, _):
-            for role, index in relays:
-                advance_at(step, role, index)
+            for role, *steps in relays:
+                advance_at(step, role, *steps)
 
             def term(place):
                 matrix = weights[2, :, place].reshape(quarter, block)
@@ -867,8 +890,8 @@
 
     def lift(which, token_block, *relays):
         def body(step, _):
-            for role, index in relays:
-                advance_at(step, role, index)
+            for role, *steps in relays:
+                advance_at(step, role, *steps)
             matrix = weights[3 + step // 2, step % 2].reshape(width, block)
             total = jnp.dot(normed_mid[token_block], matrix, preferred_element_type=jnp.float32)
             lanes = pl.ds(pl.multiple_of(step * block, block), block)
@@ -1105,11 +1128,17 @@
     return pl.pallas_call(
         whole_kernel,
         out_shape=jax.ShapeDtypeStruct((tokens, half_width), half_type),
-        in_specs=[anywhere] * 2 + [vmem] * 6 + [anywhere] * 5,
+        in_specs=[anywhere] * 13,
         out_specs=vmem,
         scratch_shapes=[
             pltpu.VMEM((tokens, half_width), half_type),
             pltpu.VMEM((tokens, half_width), full_type),
+            pltpu.VMEM((width // LANES, LANES), full_type),
+            pltpu.VMEM((width // LANES, LANES), full_type),
+            pltpu.VMEM(causal_filter_weight.shape, half_type),
+            pltpu.VMEM(decay_gate_matrix.shape, half_type),
+            pltpu.VMEM(input_gate_matrix.shape, half_type),
+            pltpu.VMEM((half_width // LANES, LANES), full_type),
             pltpu.VMEM((half_width // LANES, LANES), full_type),
             pltpu.VMEM((chunks, 2, n_fs, block, block), half_type),
             pltpu.VMEM((2, tokens, width), half_type),
@@ -1142,7 +1171,7 @@
             dma((2 * raises + 5,)),
             dma((23,)),
             dma((23,)),
-            dma((2,)),
+            dma((8,)),
         ],
         compiler_params=pltpu.CompilerParams(
             collective_id=0, has_side_effects=True, vmem_limit_bytes=67043328

time: 188 us -> 185 us (0.984)
  Pallas kernels: 186 us -> 182 us
    pallas_call x1, Pallas kernels: 186 us -> 182 us  [whole_layer(): pl.pallas_call(whole_kernel, out_shape=jax.ShapeDtypeStruct((tokens, half...]
where the time goes in v4:
time: 185 us
  Pallas kernels  182 us (98%)
  local copies, waits for them, and re-layouts  2.26 us (1%)
    pallas_call x1, Pallas kernels, whole_layer(): pl.pallas_call(whole_kernel, out_shape=jax.ShapeDtypeStruct((tokens, half...  182 us

profile of v4, /device:TPU:0, one launch (start us, length us, event | category | flops | bytes accessed | tf_op | source)
XLA Modules:
  0.0 184.5 jit_solution(12779615063552671892)
XLA Ops:
  0.0 182.3 %whole_layer.1 = bf16[512,1024]{1,0:T(8,128)(2,1)} custom-call(bf16[512,1024]{1,0:T(8,128)(2,1)} %stream_hbm.1, f32[512,1024]{1,0:T(8,128)} %offset_hbm.1, f32[16,128]{1,0:T(8,128)} %bitcast.3, f32[16,128]{1,0:T(8,128)} %bitcast.4, bf16[4,1024]{1,0:T(4,128)(2,1)} %taps_hbm.1, bf16[16,64,64]{2,1,0:T(8,128)(2,1)} %decay_maps_hbm.1, ...), custom_call_target="tpu_custom_call" | custom-call | tf_op jit(solution)/shard_map/whole_layer/pallas_call | solution.py:1128
  182.3 2.3 %copy.15 = bf16[512,1024]{1,0:T(8,128)(2,1)} copy(bf16[512,1024]{1,0:T(8,128)(2,1)} %whole_layer.1) | data formatting | bytes 2097152

commit v5 on v4

--- a/solution.py
+++ b/solution.py
@@ -319,7 +319,7 @@
 CHUNK_ROWS = 128
 AHEAD = (1, 1, 1, 1, 2, 3)
 STEADY = 4
-LEAD = 2
+LEAD = 1
 END_ORDER = (
     (0, 1), (0, 2), (0, 3), (1, 2), (1, 1), (1, 3), (2, 2), (2, 1), (2, 3), (3, 2), (3, 1), (3, 3),
 )
@@ -461,10 +461,12 @@
     def y_slot(k, q):
         return k if q == 0 else chunks + group_of(k)
 
-    def x_slot(k, h, m):
+    def x_slot(k, h, m, half=None):
         if k < last_raise:
             return group_of(k) if k < 3 else k - 1
-        return 2 + raises + (0 if h == 0 else m - 1 if m > 1 else 3 + k - last_raise)
+        if half is not None:
+            return 5 + raises + (0 if half == 0 else 1 if k < chunks - 1 else 2)
+        return 2 + raises + (0 if h == 0 else m - 1)
 
     def count_wait(ref, sem):
         pltpu.make_async_copy(ref, ref, sem).wait()
@@ -475,25 +477,32 @@
             shard_block(k, 1 - y, part), weights.at[k, part, fs], y_send.at[0], y_recv.at[y_slot(k, q)], y_peer
         )
 
-    def z_copy(k, h, m):
-        spot = weights.at[k, rep, fs if h == 0 else 2 * z + 1 - y]
+    def cut(place, k, half):
+        if half is None:
+            return weights.at[k, rep, place]
+        return weights.at[k, rep, place, :, half * (block // 2) : (half + 1) * (block // 2)]
+
+    def z_copy(k, h, m, half=None):
+        spot = cut(fs if h == 0 else 2 * z + 1 - y, k, half)
         src = shard_block(k, y, rep) if h == 0 else spot
-        return remote(src, spot, z_send.at[0], z_recv.at[k, h, m - 1], z_peer(m))
+        slot = 3 if half else m - 1
+        return remote(src, spot, z_send.at[0], z_recv.at[k, h, slot], z_peer(m))
 
     def z_relay(k, h):
         spot = weights.at[k, rep, 2 * plane(2) + (y if h == 0 else 1 - y)]
         return remote(spot, spot, z_send.at[0], z_recv.at[k, h, 2], z_peer(1))
 
-    def x_copy(k, h, m):
-        spot = weights.at[k, rep, 2 * plane(m) + (y if h == 0 else 1 - y)]
-        return remote(spot, spot, x_send.at[0], x_recv.at[x_slot(k, h, m)], x_peer)
+    def x_copy(k, h, m, half=None):
+        spot = cut(2 * plane(m) + (y if h == 0 else 1 - y), k, half)
+        return remote(spot, spot, x_send.at[0], x_recv.at[x_slot(k, h, m, half)], x_peer)
 
     every = (2, 1, 3)
     up = 6
-    events = [(k, h, every) for k, h in ((0, 0), (1, 0), (0, 1), (1, 1), (2, 0), (2, 1))]
-    events += [(k, h, every) for h in range(2) for k in range(3, last_raise)]
-    events += [(k, 0, every) for k in lowers]
-    events += [(k, 1, (2, 3)) for k in lowers] + [(k, 1, (1,)) for k in lowers]
+    events = [(k, h, every, None) for k, h in ((0, 0), (1, 0), (0, 1), (1, 1), (2, 0), (2, 1))]
+    events += [(k, h, every, None) for h in range(2) for k in range(3, last_raise)]
+    events += [(k, 0, every, None) for k in lowers]
+    events += [(k, 1, (2, 3), None) for k in lowers]
+    events += [(k, 1, (1,), half) for half in range(2) for k in lowers]
 
     def start_after(index):
         def reach_of(place):
@@ -512,7 +521,7 @@
     def start(index):
         if index >= len(events):
             return
-        k, h, sources = events[index]
+        k, h, sources, half = events[index]
         if h == 1 and 2 in sources:
             y_copy(k, 0).wait_recv()
         for m in sources:
@@ -520,7 +529,7 @@
 
                 @pl.when(is_end)
                 def _():
-                    z_copy(k, h, 1).start()
+                    z_copy(k, h, 1, half).start()
 
             elif m < 3:
                 z_copy(k, h, m).start()
@@ -531,24 +540,26 @@
                     z_copy(k, h, 3).start()
 
     def relay(index, m):
-        k, h, _ = events[index]
-        z_copy(k, h, m).wait_recv()
-        x_copy(k, h, m).start()
+        k, h, _, half = events[index]
+        z_copy(k, h, m, half).wait_recv()
+        x_copy(k, h, m, half).start()
 
         @pl.when(jnp.logical_and(is_mid, m == 2))
         def _():
             z_relay(k, h).start()
             lead = index + (1 if index < STEADY else LEAD)
-            for place in (lead,) if index != STEADY else (lead - 1, lead):
-                next_k, next_h, next_sources = events[min(place, len(events) - 1)]
+            for place in (lead,):
+                next_k, next_h, next_sources, _ = events[min(place, len(events) - 1)]
                 if next_sources == every:
                     z_copy(next_k, next_h, 1).start()
             far_step = index - up - 3 * raises
             if far_step == raises - 2:
-                z_copy(last_raise, 1, 1).start()
+                z_copy(last_raise, 1, 1, 0).start()
             if far_step == raises - 1:
                 for later_k in range(last_raise + 1, chunks):
-                    z_copy(later_k, 1, 1).start()
+                    z_copy(later_k, 1, 1, 0).start()
+                for later_k in lowers:
+                    z_copy(later_k, 1, 1, 1).start()
 
     def advance(index):
         for place, m in enumerate(sorted(events[index][2])):
@@ -957,7 +968,7 @@
     def finish(h, m):
         @pl.when(is_owner(m))
         def _():
-            (last_part(1) if (h, m) == (1, 1) else owner_copy(h, m)).wait_recv()
+            owner_copy(h, m).wait_recv()
 
             def body(step, _):
                 rows = pl.ds(pl.multiple_of(step * CHUNK_ROWS, CHUNK_ROWS), CHUNK_ROWS)
@@ -970,34 +981,95 @@
             lax.fori_loop(0, tokens // CHUNK_ROWS, body, 0)
             last_copy(h, m).start()
 
-    def last_part(which):
-        return tp_copy(partial.at[1, 1, which], partial_got.at[1, 1, which], 17 if which else 22)
+    def lanes_of(half):
+        return slice(half * (block // 2), (half + 1) * (block // 2))
+
+    def last_part(half, which):
+        lanes = lanes_of(half)
+        return tp_copy(
+            partial.at[1, 1, which, :, lanes],
+            partial_got.at[1, 1, which, :, lanes],
+            (17, 22, 23, 24)[2 * half + which],
+        )
+
+    def last_half(half):
+        lanes = lanes_of(half)
+        return remote(
+            last_send.at[1, 1, :, lanes],
+            last_got.at[1, 0, :, lanes],
+            act_send.at[(21, 25)[half]],
+            act_recv.at[(20, 25)[half]],
+            y_peer,
+        )
+
+    def half_wait(first, last, half):
+        sample = weights.at[first:last, 0, 0, :, lanes_of(0)]
+        count_wait(sample, x_recv.at[x_slot(first, 1, 1, half)])
+
+    def send_half(half):
+        lanes = lanes_of(half)
+
+        @pl.when(low)
+        def _():
+            last_part(half, 1).wait_recv()
+
+            def body(step, _):
+                rows = pl.ds(pl.multiple_of(step * CHUNK_ROWS, CHUNK_ROWS), CHUNK_ROWS)
+                last_send[1, 1, rows, lanes] = (
+                    partial[1, 1, 1, rows, lanes].astype(jnp.float32)
+                    + partial_got[1, 1, 1, rows, lanes].astype(jnp.float32)
+                ).astype(jnp.bfloat16)
+                return 0
+
+            lax.fori_loop(0, tokens // CHUNK_ROWS, body, 0)
+            last_half(half).start()
+
+    def store_half(half, which, value):
+        partial[1, 1, which, :, lanes_of(half)] = value.astype(jnp.bfloat16)
+
+        @pl.when(jnp.logical_not(low))
+        def _():
+            last_part(half, which).start()
 
     def lower_last():
         place = 2 * plane(1) + 1 - y
         split = (raises - 1) * quarter
-        for k in range(last_raise, chunks - 1):
-            wait_x(k, k + 1, 1, (1,))
+        advance(near + 2 * raises - 1)
+        half_wait(last_raise, chunks, 0)
+        for which in (1, 0):
+            matrix = weights[last_raise:chunks, :, place, :, lanes_of(0)].reshape(depth, block // 2)
+            store_half(0, which, jnp.dot(activity[which], matrix, preferred_element_type=jnp.float32))
+        send_half(0)
+        half_wait(last_raise, chunks - 1, 1)
 
         def early(which, _):
-            matrix = weights[last_raise : chunks - 1, :, place].reshape(split, block)
+            matrix = weights[last_raise : chunks - 1, :, place, :, lanes_of(1)].reshape(split, block // 2)
             total[which] = jnp.dot(activity[which, :, :split], matrix, preferred_element_type=jnp.float32)
             return 0
 
         lax.fori_loop(0, 2, early, 0)
-        wait_x(chunks - 1, chunks, 1, (1,))
+        half_wait(chunks - 1, chunks, 1)
         for which in (1, 0):
-            matrix = weights[chunks - 1, :, place].reshape(quarter, block)
+            matrix = weights[chunks - 1, :, place, :, lanes_of(1)].reshape(quarter, block // 2)
             term = jnp.dot(activity[which, :, split:], matrix, preferred_element_type=jnp.float32)
-            partial[1, 1, which] = (total[which] + term).astype(jnp.bfloat16)
+            store_half(1, which, total[which] + term)
+        send_half(1)
+
+    def close(h, mm):
+        owned = mm + 2 * (1 - low.astype(jnp.int32))
+        if (h, mm) == (0, 1):
+
+            @pl.when(low)
+            def _():
+                last_half(0).wait_recv()
+                last_half(1).wait_recv()
 
             @pl.when(jnp.logical_not(low))
             def _():
-                last_part(which).start()
-
-    def close(h, mm):
-        owned = mm + 2 * (1 - low.astype(jnp.int32))
-        last_copy(1 - h, mm).wait_recv()
+                last_copy(1, 3).wait_recv()
+
+        else:
+            last_copy(1 - h, mm).wait_recv()
         place = 2 * ((z % 2 + mm) % 2) + (y if h == 0 else 1 - y)
         lanes = pl.ds(pl.multiple_of(place * block, block), block)
 
@@ -1046,12 +1118,12 @@
 
         if index in (2, 4):
             advance_for(is_end, far + index // 2)
-        if index >= 5:
-            advance(near + index - 5)
         if (h, m) == (1, 1):
             lower_last()
-            finish(1, 1)
             continue
+        if index >= 5:
+            for step in range(raises) if index == 5 else range(raises, 2 * raises - 1):
+                advance(near + step)
         if h == 1 and m:
             wait_x(last_raise, chunks, 1, (m,))
         lower(h, m)
@@ -1065,7 +1137,8 @@
 
     @pl.when(low)
     def _():
-        last_part(0).wait_recv()
+        last_part(0, 0).wait_recv()
+        last_part(1, 0).wait_recv()
 
     close(1, 1)
     close(0, 1)
@@ -1083,7 +1156,7 @@
     for phase in range(2):
         square_copy(phase).wait_send()
         mix_copy(phase).wait_send()
-    for h, m in order:
+    for h, m in order[:-1]:
 
         @pl.when(is_owner(m))
         def _():
@@ -1091,11 +1164,18 @@
 
         @pl.when(jnp.logical_not(is_owner(m)))
         def _():
-            if (h, m) == (1, 1):
-                last_part(0).wait_send()
-                last_part(1).wait_send()
-            else:
-                owner_copy(h, m).wait_send()
+            owner_copy(h, m).wait_send()
+
+    @pl.when(low)
+    def _():
+        for half in range(2):
+            last_half(half).wait_send()
+
+    @pl.when(jnp.logical_not(low))
+    def _():
+        for half in range(2):
+            for which in range(2):
+                last_part(half, which).wait_send()
 
 
 def whole_layer(
@@ -1159,18 +1239,18 @@
             pltpu.VMEM((2, tokens, depth), half_type),
             pltpu.VMEM((4, 2, 2, tokens, block), half_type),
             pltpu.VMEM((2, 2, 2, tokens, block), half_type),
-            pltpu.VMEM((2, tokens, block), full_type),
+            pltpu.VMEM((2, tokens, block // 2), full_type),
             pltpu.VMEM((2, 2, tokens, block), half_type),
             pltpu.VMEM((2, 2, tokens, block), half_type),
             dma((1,)),
             dma((1,)),
             dma((chunks + 4,)),
             dma((1,)),
-            dma((chunks, 2, 3)),
+            dma((chunks, 2, 4)),
             dma((1,)),
-            dma((2 * raises + 5,)),
-            dma((23,)),
-            dma((23,)),
+            dma((raises + 8,)),
+            dma((26,)),
+            dma((26,)),
             dma((8,)),
         ],
         compiler_params=pltpu.CompilerParams(

time: 185 us -> 182 us (0.984)
  Pallas kernels: 182 us -> 180 us
    pallas_call x1, Pallas kernels: 182 us -> 180 us  [whole_layer(): pl.pallas_call(whole_kernel, out_shape=jax.ShapeDtypeStruct((tokens, half...]
where the time goes in v5:
time: 182 us
  Pallas kernels  180 us (99%)
  local copies, waits for them, and re-layouts  2.26 us (1%)
    pallas_call x1, Pallas kernels, whole_layer(): pl.pallas_call(whole_kernel, out_shape=jax.ShapeDtypeStruct((tokens, half...  180 us

profile of v5, /device:TPU:0, one launch (start us, length us, event | category | flops | bytes accessed | tf_op | source)
XLA Modules:
  0.0 182.0 jit_solution(3494194160483576616)
XLA Ops:
  0.0 179.8 %whole_layer.1 = bf16[512,1024]{1,0:T(8,128)(2,1)} custom-call(bf16[512,1024]{1,0:T(8,128)(2,1)} %stream_hbm.1, f32[512,1024]{1,0:T(8,128)} %offset_hbm.1, f32[16,128]{1,0:T(8,128)} %bitcast.3, f32[16,128]{1,0:T(8,128)} %bitcast.4, bf16[4,1024]{1,0:T(4,128)(2,1)} %taps_hbm.1, bf16[16,64,64]{2,1,0:T(8,128)(2,1)} %decay_maps_hbm.1, ...), custom_call_target="tpu_custom_call" | custom-call | tf_op jit(solution)/shard_map/whole_layer/pallas_call | solution.py:1208
  179.8 2.3 %copy.15 = bf16[512,1024]{1,0:T(8,128)(2,1)} copy(bf16[512,1024]{1,0:T(8,128)(2,1)} %whole_layer.1) | data formatting | bytes 2097152

commit v6 on v5

--- a/solution.py
+++ b/solution.py
@@ -485,18 +485,18 @@
     def z_copy(k, h, m, half=None):
         spot = cut(fs if h == 0 else 2 * z + 1 - y, k, half)
         src = shard_block(k, y, rep) if h == 0 else spot
-        slot = 3 if half else m - 1
-        return remote(src, spot, z_send.at[0], z_recv.at[k, h, slot], z_peer(m))
+        slot = 6 * chunks + k - last_raise if half else 6 * k + 3 * h + m - 1
+        return remote(src, spot, z_send.at[0], z_recv.at[slot], z_peer(m))
 
     def z_relay(k, h):
         spot = weights.at[k, rep, 2 * plane(2) + (y if h == 0 else 1 - y)]
-        return remote(spot, spot, z_send.at[0], z_recv.at[k, h, 2], z_peer(1))
+        return remote(spot, spot, z_send.at[0], z_recv.at[6 * k + 3 * h + 2], z_peer(1))
 
     def x_copy(k, h, m, half=None):
         spot = cut(2 * plane(m) + (y if h == 0 else 1 - y), k, half)
         return remote(spot, spot, x_send.at[0], x_recv.at[x_slot(k, h, m, half)], x_peer)
 
-    every = (2, 1, 3)
+    every = (2, 3, 1)
     up = 6
     events = [(k, h, every, None) for k, h in ((0, 0), (1, 0), (0, 1), (1, 1), (2, 0), (2, 1))]
     events += [(k, h, every, None) for h in range(2) for k in range(3, last_raise)]
@@ -1246,7 +1246,7 @@
             dma((1,)),
             dma((chunks + 4,)),
             dma((1,)),
-            dma((chunks, 2, 4)),
+            dma((6 * chunks + raises,)),
             dma((1,)),
             dma((raises + 8,)),
             dma((26,)),

time: 182 us -> 182 us (level)
  no operation moved by 1% of the time
where the time goes in v6:
time: 182 us
  Pallas kernels  180 us (99%)
  local copies, waits for them, and re-layouts  2.26 us (1%)
    pallas_call x1, Pallas kernels, whole_layer(): pl.pallas_call(whole_kernel, out_shape=jax.ShapeDtypeStruct((tokens, half...  180 us

profile of v6, /device:TPU:0, one launch (start us, length us, event | category | flops | bytes accessed | tf_op | source)
XLA Modules:
  0.0 181.9 jit_solution(15937324734094423436)
XLA Ops:
  0.0 179.6 %whole_layer.1 = bf16[512,1024]{1,0:T(8,128)(2,1)} custom-call(bf16[512,1024]{1,0:T(8,128)(2,1)} %stream_hbm.1, f32[512,1024]{1,0:T(8,128)} %offset_hbm.1, f32[16,128]{1,0:T(8,128)} %bitcast.3, f32[16,128]{1,0:T(8,128)} %bitcast.4, bf16[4,1024]{1,0:T(4,128)(2,1)} %taps_hbm.1, bf16[16,64,64]{2,1,0:T(8,128)(2,1)} %decay_maps_hbm.1, ...), custom_call_target="tpu_custom_call" | custom-call | tf_op jit(solution)/shard_map/whole_layer/pallas_call | solution.py:1208
  179.6 2.3 %copy.15 = bf16[512,1024]{1,0:T(8,128)(2,1)} copy(bf16[512,1024]{1,0:T(8,128)(2,1)} %whole_layer.1) | data formatting | bytes 2097152
